TPU v7x, 32 devices: a whole 2x2x4 slice. The times are simulated.
32 devices in a mesh: ep: 16 (over z, x, core), tp: 2 (over y).
Axes of the slice: x: 2, y: 2, z: 4, core: 2. Of those that a mesh axis runs over, the one named last changes fastest.
Arguments:
- tokens: bfloat16 [256, 2048], P('ep'), may hold values from -6 to 6
- attn_gain: bfloat16 [2048], replicated, may hold values from 0.099609375 to 1.8984375
- query_weight: bfloat16 [2048, 1024], P('ep', 'tp'), may hold values from -0.125 to 0.125
- key_weight: bfloat16 [2048, 512], P('ep', 'tp'), may hold values from -0.125 to 0.125
- value_weight: bfloat16 [2048, 512], P('ep', 'tp'), may hold values from -0.125 to 0.125
- out_weight: bfloat16 [2048, 1024], P('ep', 'tp'), may hold values from -0.1875 to 0.1875
- head_gain: bfloat16 [1024], P('tp'), may hold values from 0.099609375 to 1.8984375
- past_keys: bfloat16 [256, 1024, 4, 128], P('ep', None, 'tp'), may hold values from -6 to 6
- past_values: bfloat16 [256, 1024, 4, 128], P('ep', None, 'tp'), may hold values from -50 to 50
- break_offset: float32 [256, 8, 1024], P('ep', 'tp'), may hold values from -12.5 to 1
- cache_lengths: int32 [256], P('ep'), may hold values from 1 to 1024, 131072 in all
- ffn_gain: bfloat16 [2048], replicated, may hold values from 0.099609375 to 1.8984375
- router_weight: bfloat16 [2048, 16], replicated, may hold values from -0.25 to 0.25
- expert_routes: int32 [256, 6], P('ep'), may hold values from 0 to 15, all different within a row; in each aligned block of 16 rows (0 to 15, 16 to 31, ...) at most 12 rows name the same one
- expert_gate: bfloat16 [16, 2048, 512], P('ep', None, 'tp'), may hold values from -0.125 to 0.125
- expert_up: bfloat16 [16, 2048, 512], P('ep', None, 'tp'), may hold values from -0.125 to 0.125
- expert_down: bfloat16 [16, 512, 2048], P('ep', 'tp'), may hold values from -0.25 to 0.25
- shared_gate: bfloat16 [2048, 512], P(None, 'tp'), may hold values from -0.125 to 0.125
- shared_up: bfloat16 [2048, 512], P(None, 'tp'), may hold values from -0.125 to 0.125
- shared_down: bfloat16 [512, 2048], P('tp'), may hold values from -0.25 to 0.25
Outputs:
- mixed: bfloat16 [256, 2048], P('ep', 'tp')
- fresh_keys: bfloat16 [256, 512], P('ep', 'tp')
- fresh_values: bfloat16 [256, 512], P('ep', 'tp')
Inputs may be any that keep to these rules, and one draw needn't show every extreme that they name: `cache_lengths`: the lengths add up to half of 262144, and some sequence has length 1024. `expert_routes`: each row names 6 different experts. Among the rows of one device no expert is named more than 12 times, and 12 is reached in some device's rows.
All inputs are finite; a program needn't handle non-finite values. No bound on the sum of `cache_lengths` on one device may be relied on, other than what follows from the above.
Results may differ from a plain program's by a relative error of at most 0.0095.
Values may be sent and summed in bfloat16 or wider, within the bound.
No kernel may reach another device: no remote copies, remote signals or barrier semaphores. Data moves between devices by JAX's collectives and lax.ppermute only.
A program may use at most 64 MiB of HBM per device.

v0:
```python
import jax
import jax.numpy as jnp
from jax import lax
from jax.experimental import pallas as pl
from jax.experimental.pallas import tpu as pltpu
from jax.sharding import PartitionSpec as P


epsilon = 1e-06
routed_scale = 2.5
LANES = 128
bf16 = jnp.bfloat16
f32 = jnp.float32


def dot(a, b, dims=((1,), (0,)), precision=None):
    return lax.dot_general(a, b, (dims, ((), ())), precision=precision, preferred_element_type=f32)


def split3(value):
    high = value.astype(bf16)
    rest = value - high.astype(f32)
    mid = rest.astype(bf16)
    low = (rest - mid.astype(f32)).astype(bf16)
    return high, mid, low


def split2(value):
    high = value.astype(bf16)
    return high, (value - high.astype(f32)).astype(bf16)


def attend_kernel(lengths, q_ref, k_ref, v_ref, off_ref, gain_ref, out_ref, heads_ref, *, seqs, heads, key_heads):
    step = pl.program_id(0)
    rows = k_ref.shape[1]
    head_size = k_ref.shape[2]
    half = rows // 2
    positions = rows // key_heads
    block = LANES * key_heads
    group = heads // key_heads
    both = 2 * heads
    blocks = half // LANES
    off_blocks = positions // 2 // LANES
    row = lax.broadcasted_iota(jnp.int32, (both, half), 0)
    col = lax.broadcasted_iota(jnp.int32, (both, half), 1)
    place = jnp.where(row >= heads, positions // 2, 0) + col // key_heads
    mine = (col % key_heads) == ((row % heads) // group)
    low_row = row < heads
    scale = head_size ** (-0.5)
    spread = (
        lax.broadcasted_iota(jnp.int32, (LANES, block), 1) // key_heads
        == lax.broadcasted_iota(jnp.int32, (LANES, block), 0)
    ).astype(bf16)
    tri_row = lax.broadcasted_iota(jnp.int32, (LANES, 2 * LANES), 0)
    tri_col = lax.broadcasted_iota(jnp.int32, (LANES, 2 * LANES), 1)
    tri = ((tri_row > tri_col) | (tri_col >= LANES)).astype(bf16)

    scores = []
    for s in range(seqs):
        own = q_ref[pl.ds(step * seqs + s, 1), :]
        heads_q = jnp.concatenate([own[:, h * head_size : (h + 1) * head_size] for h in range(heads)] * 2, axis=0)
        q8 = heads_q.astype(bf16)
        s_lo = dot(q8, k_ref[s, :half, :], ((1,), (1,)))
        s_hi = dot(q8, k_ref[s, half:, :], ((1,), (1,)))
        scores.append(jnp.where(low_row, s_lo, s_hi) * scale)
    stacked = []
    for s in range(seqs):
        off = off_ref[s]
        off8 = jnp.concatenate([off[:, : positions // 2], off[:, positions // 2 :]], axis=0)
        stacked += [off8[:, b * LANES : (b + 1) * LANES] for b in range(off_blocks)]
    high, low = split2(jnp.concatenate(stacked, axis=0))
    wide = dot(high, spread) + dot(low, spread)
    keep_rows, valids, stops = [], [], []
    for s in range(seqs):
        start = s * off_blocks
        offsets = jnp.concatenate(
            [wide[(start + b) * both : (start + b + 1) * both] for b in range(off_blocks)], axis=1
        )
        logits = scores[s] + offsets
        valid = mine & (place < lengths[step * seqs + s])
        tail = jnp.log(1.0 + jnp.exp(-jnp.abs(logits)))
        stops.append(jnp.minimum(logits, 0.0) - tail)
        keep = jnp.where(valid, -jnp.maximum(logits, 0.0) - tail, 0.0)
        keep_rows += [keep[:, b * LANES : (b + 1) * LANES] for b in range(blocks)]
        valids.append(valid)
    high, low = split2(jnp.concatenate(keep_rows, axis=0))
    sums = dot(high, tri) + dot(low, tri)
    top_row = lax.broadcasted_iota(jnp.int32, (both, LANES), 0) < heads
    for s in range(seqs):
        after = [None] * blocks
        running = jnp.zeros((both, LANES), f32)
        for b in reversed(range(blocks)):
            base = (s * blocks + b) * both
            after[b] = sums[base : base + both, :LANES] + running
            running = running + sums[base : base + both, LANES:]
        upper = jnp.where(top_row, pltpu.roll(running, heads, 0), 0.0)
        after_sum = jnp.concatenate([a + upper for a in after], axis=1)
        sticks = jnp.where(valids[s], jnp.exp(stops[s] + after_sum), 0.0).astype(bf16)
        o_lo = dot(sticks, v_ref[s, :half, :])
        o_hi = dot(sticks, v_ref[s, half:, :])
        out = o_lo + pltpu.roll(o_hi, heads, 0)
        for h in range(heads):
            heads_ref[step, s : s + 1, h * head_size : (h + 1) * head_size] = out[h : h + 1]

    @pl.when(step == pl.num_programs(0) - 1)
    def _():
        values = jnp.concatenate([heads_ref[i] for i in range(heads_ref.shape[0])], axis=0)
        width = values.shape[1]
        out_ref[:, :width] = (values * gain_ref[...].astype(f32)).astype(bf16)
        square = jnp.sum(values * values, axis=1, keepdims=True)
        first, second, third = [p.astype(f32) for p in split3(square)]
        lane = lax.broadcasted_iota(jnp.int32, (values.shape[0], LANES), 1)
        extra = jnp.where(lane == 0, first, jnp.where(lane == 1, second, jnp.where(lane == 2, third, 0.0)))
        out_ref[:, width:] = extra.astype(bf16)


def load_kernel(lengths, cache_hbm, out_ref, sem, *, key_heads, chunk, clear):
    count, rows, head_size = out_ref.shape
    per = chunk * key_heads
    chunks = rows // per

    def window(c):
        return pl.ds(pl.multiple_of(c * per, per), per)

    def copy(s, c):
        return pltpu.make_async_copy(cache_hbm.at[s, window(c)], out_ref.at[s, window(c)], sem)

    def live(s):
        return (lengths[s] + chunk - 1) // chunk

    @pl.loop(0, count)
    def _(s):
        @pl.loop(0, live(s))
        def _(c):
            copy(s, c).start()

    if clear:

        @pl.loop(0, count)
        def _(s):
            @pl.loop(live(s), chunks)
            def _(c):
                out_ref[s, window(c), :] = jnp.zeros((per, head_size), bf16)

    @pl.loop(0, count)
    def _(s):
        @pl.loop(0, live(s))
        def _(c):
            copy(s, c).wait()


def load(cache, lengths, clear, limit):
    seq_count, positions, key_heads, head_size = cache.shape
    rows = positions * key_heads
    shape = (seq_count, rows, head_size)

    def kernel(*refs):
        load_kernel(*refs, key_heads=key_heads, chunk=min(positions, 256), clear=clear)

    return pl.pallas_call(
        kernel,
        out_shape=pltpu.VMEM(shape, bf16),
        in_specs=[pl.BlockSpec(memory_space=pltpu.SMEM), pl.BlockSpec(memory_space=pltpu.HBM)],
        out_specs=pl.BlockSpec(memory_space=pltpu.VMEM),
        scratch_shapes=[pltpu.SemaphoreType.DMA(())],
        compiler_params=pltpu.CompilerParams(vmem_limit_bytes=limit * 1024 * 1024),
        name="load_cache",
    )(lengths, pltpu.with_memory_space_constraint(cache.reshape(shape), pltpu.HBM))


def load_weights(weights):
    def kernel(*refs):
        count = len(weights)
        sources, targets, sems = refs[:count], refs[count : 2 * count], refs[-1]
        copies = [pltpu.make_async_copy(a, b, sems.at[i]) for i, (a, b) in enumerate(zip(sources, targets))]
        for copy in copies:
            copy.start()
        for copy in copies:
            copy.wait()

    return pl.pallas_call(
        kernel,
        out_shape=tuple(pltpu.VMEM(w.shape, w.dtype) for w in weights),
        in_specs=[pl.BlockSpec(memory_space=pltpu.HBM)] * len(weights),
        out_specs=tuple(pl.BlockSpec(memory_space=pltpu.VMEM) for _ in weights),
        scratch_shapes=[pltpu.SemaphoreType.DMA((len(weights),))],
        compiler_params=pltpu.CompilerParams(vmem_limit_bytes=4 * 1024 * 1024),
        name="load_weights",
    )(*[pltpu.with_memory_space_constraint(w, pltpu.HBM) for w in weights])


def merge_kernel(starts, kept_ref, other_ref, shared_ref, keep_ref, send_ref):
    _, cols = keep_ref.shape
    seqs = shared_ref.shape[0]
    for target, i in ((send_ref, 1), (keep_ref, 0)):
        window = pl.ds(pl.multiple_of(starts[i], LANES), cols)
        total = kept_ref[:, window].astype(f32) + other_ref[:, window].astype(f32)
        first = total[:seqs] + shared_ref[:, window]
        target[...] = jnp.concatenate([first, total[seqs:]], axis=0).astype(target.dtype)


def merge(starts, kept, other, shared, cols):
    rows = kept.shape[0]
    return pl.pallas_call(
        merge_kernel,
        out_shape=(jax.ShapeDtypeStruct((rows, cols), f32), jax.ShapeDtypeStruct((rows, cols), bf16)),
        grid_spec=pltpu.PrefetchScalarGridSpec(
            num_scalar_prefetch=1,
            grid=(1,),
            in_specs=[whole(kept.shape), whole(other.shape), whole(shared.shape)],
            out_specs=(whole((rows, cols)), whole((rows, cols))),
        ),
        compiler_params=pltpu.CompilerParams(vmem_limit_bytes=8 * 1024 * 1024),
        name="merge",
    )(starts, kept, other, shared)


def attend(queries, keys, values, offsets, lengths, head_gain):
    seq_count, rows, head_size = keys.shape
    heads, positions = offsets.shape[1:]
    key_heads = rows // positions
    seqs = 4
    width = heads * head_size

    def kernel(*refs):
        attend_kernel(*refs, seqs=seqs, heads=heads, key_heads=key_heads)

    return pl.pallas_call(
        kernel,
        out_shape=jax.ShapeDtypeStruct((seq_count, width + LANES), bf16),
        grid_spec=pltpu.PrefetchScalarGridSpec(
            num_scalar_prefetch=1,
            grid=(seq_count // seqs,),
            in_specs=[
                pl.BlockSpec((seq_count, width), lambda i, n: (0, 0)),
                pl.BlockSpec((seqs, rows, head_size), lambda i, n: (i, 0, 0)),
                pl.BlockSpec((seqs, rows, head_size), lambda i, n: (i, 0, 0)),
                pl.BlockSpec((seqs, heads, positions), lambda i, n: (i, 0, 0)),
                pl.BlockSpec((1, width), lambda i, n: (0, 0)),
            ],
            out_specs=pl.BlockSpec((seq_count, width + LANES), lambda i, n: (0, 0)),
            scratch_shapes=[pltpu.VMEM((seq_count // seqs, seqs, width), f32)],
        ),
        compiler_params=pltpu.CompilerParams(
            dimension_semantics=("arbitrary",), vmem_limit_bytes=20 * 1024 * 1024
        ),
        cost_estimate=pl.CostEstimate(flops=2 * 10**9, transcendentals=10**6, bytes_accessed=2 * 10**7),
        name="stick_attend",
    )(
        lengths,
        queries,
        pltpu.with_memory_space_constraint(keys, pltpu.VMEM),
        pltpu.with_memory_space_constraint(values, pltpu.HBM),
        offsets,
        head_gain.reshape(1, width),
    )


def whole(shape):
    return pl.BlockSpec(shape, lambda *_: tuple(0 for _ in shape))


def project_kernel(rows_ref, *refs):
    weights, out_ref = refs[:-1], refs[-1]
    block = weights[0].shape[0]
    total = None
    for i, weight in enumerate(weights):
        piece = dot(rows_ref[:, i * block : (i + 1) * block], weight[...])
        total = piece if total is None else total + piece
    out_ref[...] = total.astype(bf16)


def project(rows, weights):
    shape = (rows.shape[0], weights[0].shape[1])
    return pl.pallas_call(
        project_kernel,
        out_shape=jax.ShapeDtypeStruct(shape, bf16),
        in_specs=[whole(rows.shape)] + [whole(w.shape) for w in weights],
        out_specs=whole(shape),
        grid=(1,),
        compiler_params=pltpu.CompilerParams(vmem_limit_bytes=8 * 1024 * 1024),
        name="project",
    )(rows, *weights)


def out_kernel(*refs, count, width, extra):
    messages, weights, out_ref = refs[:count], refs[count:-1], refs[-1]
    rows = jnp.concatenate([m[:, :width] for m in messages], axis=0)
    pieces = [dot(rows, weight[...], ((1,), (1,))).astype(bf16) for weight in weights]
    pieces.append(jnp.concatenate([m[:, width : width + extra] for m in messages], axis=0))
    out_ref[...] = jnp.concatenate(pieces, axis=1)


def out_project(messages, weights, width, extra):
    rows = sum(m.shape[0] for m in messages)
    shape = (rows, sum(w.shape[0] for w in weights) + extra)

    def kernel(*refs):
        out_kernel(*refs, count=len(messages), width=width, extra=extra)

    return pl.pallas_call(
        kernel,
        out_shape=jax.ShapeDtypeStruct(shape, bf16),
        in_specs=[whole(m.shape) for m in messages] + [whole(w.shape) for w in weights],
        out_specs=whole(shape),
        grid=(1,),
        compiler_params=pltpu.CompilerParams(vmem_limit_bytes=8 * 1024 * 1024),
        name="out_project",
    )(*messages, *weights)


def experts_kernel(place, rows_ref, gain_ref, router_ref, *refs, model, experts, groups):
    gates, ups, downs, out_ref = refs[:groups], refs[groups : 2 * groups], refs[2 * groups : 3 * groups], refs[-1]
    data = rows_ref[:, :model].astype(f32)
    factor = lax.rsqrt(jnp.sum(data * data, axis=-1, keepdims=True) * (1.0 / model) + epsilon)
    normed = (data * factor * gain_ref[...].astype(f32)).astype(bf16)
    mask = rows_ref[:, model:].astype(f32)[:, :experts]
    prob = jax.nn.sigmoid(dot(normed, router_ref[...], ((1,), (1,)))) * mask
    weight = routed_scale * prob / jnp.sum(prob, axis=-1, keepdims=True)
    lane = lax.broadcasted_iota(jnp.int32, weight.shape, 1)
    total = None
    for g in range(groups):
        for e in range(gates[g].shape[0]):
            expert = place[g] * gates[g].shape[0] + e
            mine = jnp.sum(jnp.where(lane == expert, weight, 0.0), axis=-1, keepdims=True)
            gate = dot(normed, gates[g][e])
            up = dot(normed, ups[g][e])
            hidden = (gate / (1.0 + jnp.exp(-gate)) * up).astype(bf16)
            piece = dot(hidden, downs[g][e]) * mine
            total = piece if total is None else total + piece
    out_ref[...] = total.astype(bf16)


def run_experts(rows, gain, router, gates, ups, downs, place):
    count = rows.shape[0]
    model = gates[0].shape[1]
    shape = (count, model)

    def kernel(*refs):
        experts_kernel(*refs, model=model, experts=router.shape[0], groups=len(gates))

    return pl.pallas_call(
        kernel,
        out_shape=jax.ShapeDtypeStruct(shape, bf16),
        grid_spec=pltpu.PrefetchScalarGridSpec(
            num_scalar_prefetch=1,
            grid=(1,),
            in_specs=[whole(rows.shape), whole((1, model)), whole(router.shape)]
            + [pl.BlockSpec(memory_space=pltpu.VMEM)] * (3 * len(gates)),
            out_specs=whole(shape),
        ),
        compiler_params=pltpu.CompilerParams(vmem_limit_bytes=12 * 1024 * 1024),
        name="routed_experts",
    )(
        place,
        rows,
        gain.reshape(1, model),
        router,
        *[pltpu.with_memory_space_constraint(w, pltpu.VMEM) for w in (*gates, *ups, *downs)],
    )


def make_body(n_ep, n_tp):
    inner = 1 << ((n_ep.bit_length() - 1) // 2)
    outer = n_ep // inner
    masks = [1 << i for i in reversed(range(inner.bit_length() - 1))]

    def swap(value, mask):
        return lax.ppermute(value, "ep", [(i, i ^ mask) for i in range(n_ep)])

    def outer_swap(value, k):
        return swap(value, k * inner)

    def tp_swap(value):
        return lax.ppermute(value, "tp", [(i, (i + 1) % n_tp) for i in range(n_tp)])

    def gather(value, over):
        pieces, order = [value], [0]
        for m in over:
            pieces = pieces + [swap(p, m) for p in pieces]
            order = order + [o ^ m for o in order]
        return pieces, order

    def reverse_bits(value):
        result, width = jnp.uint32(0), inner
        while width > 1:
            result = (result << 1) | (value & 1)
            value = value >> 1
            width = width // 2
        return result

    def cut(value, start, size):
        return lax.dynamic_slice(value, (jnp.uint32(0), start), (value.shape[0], size))

    def body(
        tokens,
        attn_gain,
        query_weight,
        key_weight,
        value_weight,
        out_weight,
        head_gain,
        past_keys,
        past_values,
        break_offset,
        cache_lengths,
        ffn_gain,
        router_weight,
        expert_routes,
        expert_gate,
        expert_up,
        expert_down,
        shared_gate,
        shared_up,
        shared_down,
    ):
        seqs, model = tokens.shape
        experts = router_weight.shape[1]
        block = query_weight.shape[0]
        plane = block * inner
        cols = model // n_tp
        key_cols = key_weight.shape[1]
        heads_width = out_weight.shape[1]
        pad = -experts % LANES

        me = lax.axis_index("ep").astype(jnp.uint32)
        my_tp = lax.axis_index("tp").astype(jnp.uint32)
        my_inner = me & (inner - 1)
        my_outer = me >> (inner.bit_length() - 1)
        marks = [my_outer ^ k for k in range(outer)]
        starts = [m * plane for m in marks]
        blocks_at = [(my_inner ^ o) * block for o in range(inner)]
        back_at = [reverse_bits(my_inner ^ o) * block for o in range(inner)]
        own_start, other_start = my_tp * cols, ((my_tp + 1) & (n_tp - 1)) * cols
        row_starts = [m * (outer * seqs) for m in marks]
        place = jnp.stack([me, me ^ 1]).astype(jnp.int32)
        col_starts = jnp.stack([own_start, other_start]).astype(jnp.int32)
        held = (tokens, starts, row_starts, blocks_at, back_at, own_start, col_starts, place)
        held = lax.optimization_barrier(held)
        tokens, starts, row_starts, blocks_at, back_at, own_start, col_starts, place = held

        query_pieces, order = gather(query_weight, masks)
        got = [cut(tokens, starts[0], plane)] + [outer_swap(cut(tokens, starts[k], plane), k) for k in range(1, outer)]
        group_tokens = jnp.concatenate(got, axis=0)

        def by_order(value):
            return jnp.concatenate([cut(value, blocks_at[o], block) for o in order], axis=1)

        gain_plane = cut(attn_gain.reshape(1, model), starts[0], plane)
        ordered = by_order(group_tokens)
        gained = (ordered.astype(f32) * by_order(gain_plane).astype(f32)).astype(bf16)
        query_part = project(gained, query_pieces)
        late = lax.optimization_barrier(
            (query_part, cache_lengths, out_weight, key_weight, value_weight, expert_gate, expert_up, expert_down)
        )
        query_part, load_lengths, out_weight, key_weight, value_weight, expert_gate, expert_up, expert_down = late
        keys = load(past_keys, load_lengths, False, 4)
        query_got = [query_part[:seqs]] + [
            outer_swap(query_part[k * seqs : (k + 1) * seqs], k) for k in range(1, outer)
        ]
        out_pieces, _ = gather(out_weight, masks)
        rest_pieces, _ = gather(jnp.concatenate([key_weight, value_weight], axis=1), masks)
        gates, ups, downs = [[w, swap(w, 1)] for w in (expert_gate, expert_up, expert_down)]
        wide_tokens = tokens.astype(f32)
        factor = lax.rsqrt(jnp.mean(wide_tokens * wide_tokens, axis=-1, keepdims=True) + epsilon)
        queries = (sum(part.astype(f32) for part in query_got) * factor).astype(bf16).astype(f32)

        lane = lax.broadcasted_iota(jnp.int32, (1, 1, experts + pad), 2)
        routed_mask = jnp.sum((expert_routes[:, :, None] == lane).astype(f32), axis=1).astype(bf16)
        rest_part = project(gained, rest_pieces)

        values = past_values.reshape(keys.shape)
        queries, gates, ups, downs = lax.optimization_barrier((queries, gates, ups, downs))
        scaled = attend(queries, keys, values, break_offset, cache_lengths, head_gain)
        messages = [
            jnp.concatenate([scaled, routed_mask, rest_part[k * seqs : (k + 1) * seqs]], axis=1)
            for k in range(outer)
        ]
        arrived = [messages[0]] + [outer_swap(messages[k], k) for k in range(1, outer)]
        cuts = (heads_width, heads_width + LANES, heads_width + LANES + experts + pad)
        group_mask = jnp.concatenate([m[:, cuts[1] : cuts[2]] for m in arrived], axis=0)
        own_part = out_project(arrived, out_pieces, heads_width, LANES)
        other_part = tp_swap(own_part)
        both = own_part.astype(f32) + other_part.astype(f32)
        square_total = jnp.sum(both[:, plane:], axis=1, keepdims=True)
        attention = both[:, :plane] * lax.rsqrt(square_total / (heads_width * n_tp) + epsilon)
        residual_part = (ordered.astype(f32) + attention).astype(bf16)

        residual_plane = jnp.concatenate([cut(residual_part, back_at[o], block) for o in range(inner)], axis=1)
        residual_plane, gates, ups, downs = lax.optimization_barrier((residual_plane, gates, ups, downs))
        held_weights = load_weights((*gates, *ups, *downs))
        gates, ups, downs = held_weights[:2], held_weights[2:4], held_weights[4:]
        peers = [residual_plane] + [outer_swap(residual_plane, k) for k in range(1, outer)]
        stacked = []
        for k in range(outer):
            stacked += [peers[k][(j ^ k) * seqs : (j ^ k) * seqs + seqs] for j in range(outer)]
        stacked = jnp.concatenate(stacked, axis=0)
        group_rows = jnp.concatenate(
            [lax.dynamic_slice(stacked, (row_starts[p], jnp.uint32(0)), (outer * seqs, plane)) for p in range(outer)]
            + [group_mask],
            axis=1,
        )
        row_pieces, _ = gather(group_rows, masks[:-1])

        arrived, group_rows = lax.optimization_barrier((arrived, group_rows))
        fresh = (sum(m[:, cuts[2] :].astype(f32) for m in arrived) * factor).astype(bf16)

        own_rows = group_rows[:seqs, :model]
        data = own_rows.astype(f32)
        scale = lax.rsqrt(jnp.mean(data * data, axis=-1, keepdims=True) + epsilon)
        own_normed = (data * scale * ffn_gain.astype(f32)).astype(bf16)
        shared_hidden = (
            jax.nn.silu(dot(own_normed, shared_gate)) * dot(own_normed, shared_up)
        ).astype(bf16)
        shared_part = dot(shared_hidden, shared_down)

        router = router_weight.T
        results = [run_experts(piece, ffn_gain, router, gates, ups, downs, place) for piece in row_pieces]

        for m in reversed(masks[1:-1]):
            half = len(results) // 2
            back = [swap(r, m) for r in results[half:]]
            results = [(a.astype(f32) + b.astype(f32)).astype(bf16) for a, b in zip(results[:half], back)]
        kept = results[0]
        other = swap(results[1], masks[0]) if len(results) > 1 else jnp.zeros_like(kept)

        keep, send = merge(col_starts, kept, other, shared_part, cols)
        value = keep + tp_swap(send).astype(f32)
        value_out = value.astype(bf16)
        total = value[:seqs]
        for k in range(1, outer):
            total = total + outer_swap(value_out[k * seqs : (k + 1) * seqs], k).astype(f32)
        mixed = (cut(own_rows, own_start, cols).astype(f32) + total).astype(bf16)
        return mixed, fresh[:, :key_cols], fresh[:, key_cols:]

    return body


def solution(mesh):
    placed = (
        P("ep", None),
        P(),
        P("ep", "tp"),
        P("ep", "tp"),
        P("ep", "tp"),
        P("ep", "tp"),
        P("tp"),
        P("ep", None, "tp", None),
        P("ep", None, "tp", None),
        P("ep", "tp", None),
        P("ep"),
        P(),
        P(),
        P("ep", None),
        P("ep", None, "tp"),
        P("ep", None, "tp"),
        P("ep", "tp", None),
        P(None, "tp"),
        P(None, "tp"),
        P("tp", None),
    )
    return jax.shard_map(
        make_body(mesh.shape["ep"], mesh.shape["tp"]),
        mesh=mesh,
        in_specs=placed,
        out_specs=(P("ep", "tp"), P("ep", "tp"), P("ep", "tp")),
        check_vma=False,
    )
```

profile of v0, /device:TPU:0, one launch (start us, length us, event | category | flops | bytes accessed | tf_op | source)
XLA Modules:
  0.0 97.4 jit_solution(5771606729715338385)
XLA Ops:
  0.6 3.0 %collective-permute-start.3 = (bf16[128,512]{1,0:T(8,128)(2,1)}, bf16[128,512]{1,0:T(8,128)(2,1)S(1)}, u32[]{:S(2)}, u32[]{:S(2)}) collective-permute-start(bf16[128,512]{1,0:T(8,128)(2,1)} %refs_0_.2), channel_id=1, source_target_pairs={{0,4},{2,6},{4,0},{6,2},{8,12},{10,14},{12,8},{14,10},{16,20},{18,... | collective-permute-start | bytes 393224 | tf_op jit(solution)/shard_map/ppermute | solution.py:369
  4.7 3.7 %collective-permute-start.2 = (bf16[16,512]{1,0:T(8,128)(2,1)S(1)}, bf16[16,512]{1,0:T(8,128)(2,1)S(1)}, u32[]{:S(2)}, u32[]{:S(2)}) collective-permute-start(bf16[16,512]{1,0:T(8,128)(2,1)S(1)} %get-tuple-element.134), channel_id=1, source_target_pairs={{0,24},{2,26},{4,28},{6,30},{8,16},{10,18},{12,20},{14,22},{16,8},... | collective-permute-start | bytes 49160 | tf_op jit(solution)/shard_map/ppermute | solution.py:369
  11.0 1.9 %collective-permute-done.1 = bf16[16,512]{1,0:T(8,128)(2,1)S(1)} collective-permute-done((bf16[16,512]{1,0:T(8,128)(2,1)S(1)}, bf16[16,512]{1,0:T(8,128)(2,1)S(1)}, u32[]{:S(2)}, u32[]{:S(2)}) %collective-permute-start.1) | collective-permute-done | bytes 16416 | tf_op jit(solution)/shard_map/ppermute | solution.py:369
  16.4 1.7 %collective-permute-start.8 = (bf16[16,512]{1,0:T(8,128)(2,1)S(1)}, bf16[16,512]{1,0:T(8,128)(2,1)S(1)}, u32[]{:S(2)}, u32[]{:S(2)}) collective-permute-start(bf16[16,512]{1,0:T(8,128)(2,1)S(1)} %get-tuple-element.127), channel_id=1, source_target_pairs={{0,24},{2,26},{4,28},{6,30},{8,16},{10,18},{12,20},{14,22},{16,8},... | collective-permute-start | bytes 49160 | tf_op jit(solution)/shard_map/ppermute | solution.py:369
  19.2 2.7 %collective-permute-done.8 = bf16[16,512]{1,0:T(8,128)(2,1)S(1)} collective-permute-done((bf16[16,512]{1,0:T(8,128)(2,1)S(1)}, bf16[16,512]{1,0:T(8,128)(2,1)S(1)}, u32[]{:S(2)}, u32[]{:S(2)}) %collective-permute-start.8) | collective-permute-done | bytes 16416 | tf_op jit(solution)/shard_map/ppermute | solution.py:369
  24.1 1.6 %collective-permute-done.6 = bf16[16,512]{1,0:T(8,128)(2,1)S(1)} collective-permute-done((bf16[16,512]{1,0:T(8,128)(2,1)S(1)}, bf16[16,512]{1,0:T(8,128)(2,1)S(1)}, u32[]{:S(2)}, u32[]{:S(2)}) %collective-permute-start.6) | collective-permute-done | bytes 16416 | tf_op jit(solution)/shard_map/ppermute | solution.py:369
  27.8 3.6 %load_cache.1.refs_2_ = bf16[16,2048,128]{2,1,0:T(8,128)(2,1)S(1)} custom-call(s32[16]{0:T(128)S(1)} %copy-done.5, bf16[16,2048,128]{2,1,0:T(8,128)(2,1)} %bitcast.12), custom_call_target="tpu_custom_call" | custom-call | tf_op jit(solution)/shard_map/load_cache/pallas_call | solution.py:160
  31.9 5.2 %collective-permute-done.18.refs_5_ = bf16[128,512]{1,0:T(8,128)(2,1)S(1)} collective-permute-done((bf16[128,512]{1,0:T(8,128)(2,1)S(1)}, bf16[128,512]{1,0:T(8,128)(2,1)S(1)}, u32[]{:S(2)}, u32[]{:S(2)}) %collective-permute-start.18) | collective-permute-done | bytes 131104 | tf_op jit(solution)/shard_map/ppermute | solution.py:369
  38.0 8.6 %stick_attend.1 = bf16[16,640]{1,0:T(8,128)(2,1)S(1)} custom-call(s32[16]{0:T(128)S(1)} %copy-done.6, f32[16,512]{1,0:T(8,128)S(1)} %fusion.11.refs_1_, bf16[16,2048,128]{2,1,0:T(8,128)(2,1)S(1)} %load_cache.1.refs_2_, bf16[16,2048,128]{2,1,0:T(8,128)(2,1)} %bitcast.13, f32[16,4,1024]{2,1,0:T(4,128)S(1)} %copy-done.1, bf16[1,512]{1,0:T(2,128)(2,1)S(1)} %reshape.95.refs_5_), custom_call_target="tpu_custom_call" | custom-call | flops 2000000000 | bytes 20000000 | tf_op jit(solution)/shard_map/stick_attend/pallas_call | solution.py:228
  46.7 1.7 %collective-permute-start.16 = (bf16[16,1280]{1,0:T(8,128)(2,1)S(1)}, bf16[16,1280]{1,0:T(8,128)(2,1)S(1)}, u32[]{:S(2)}, u32[]{:S(2)}) collective-permute-start(bf16[16,1280]{1,0:T(8,128)(2,1)S(1)} %get-tuple-element.138), channel_id=1, source_target_pairs={{0,16},{2,18},{4,20},{6,22},{8,24},{10,26},{12,28},{14,30},{16,0},... | collective-permute-start | bytes 122888 | tf_op jit(solution)/shard_map/ppermute | solution.py:369
  48.4 2.6 %collective-permute-start.17 = (bf16[16,1280]{1,0:T(8,128)(2,1)S(1)}, bf16[16,1280]{1,0:T(8,128)(2,1)S(1)}, u32[]{:S(2)}, u32[]{:S(2)}) collective-permute-start(bf16[16,1280]{1,0:T(8,128)(2,1)S(1)} %get-tuple-element.137), channel_id=1, source_target_pairs={{0,24},{2,26},{4,28},{6,30},{8,16},{10,18},{12,20},{14,22},{16,8},... | collective-permute-start | bytes 122888 | tf_op jit(solution)/shard_map/ppermute | solution.py:369
  52.1 2.1 %collective-permute-done.17.refs_3_ = bf16[16,1280]{1,0:T(8,128)(2,1)S(1)} collective-permute-done((bf16[16,1280]{1,0:T(8,128)(2,1)S(1)}, bf16[16,1280]{1,0:T(8,128)(2,1)S(1)}, u32[]{:S(2)}, u32[]{:S(2)}) %collective-permute-start.17) | collective-permute-done | bytes 40992 | tf_op jit(solution)/shard_map/ppermute | solution.py:369
  54.5 1.6 %collective-permute-start.21 = (bf16[64,640]{1,0:T(8,128)(2,1)S(1)}, bf16[64,640]{1,0:T(8,128)(2,1)S(1)}, u32[]{:S(2)}, u32[]{:S(2)}) collective-permute-start(bf16[64,640]{1,0:T(8,128)(2,1)S(1)} %out_project.1), channel_id=1, source_target_pairs={{0,1},{1,0},{2,3},{3,2},{4,5},{5,4},{6,7},{7,6},{8,9},{9,8},{10,11... | collective-permute-start | bytes 245768 | tf_op jit(solution)/shard_map/ppermute | solution.py:375
  56.2 2.9 %collective-permute-done.21 = bf16[64,640]{1,0:T(8,128)(2,1)S(1)} collective-permute-done((bf16[64,640]{1,0:T(8,128)(2,1)S(1)}, bf16[64,640]{1,0:T(8,128)(2,1)S(1)}, u32[]{:S(2)}, u32[]{:S(2)}) %collective-permute-start.21) | collective-permute-done | bytes 81952 | tf_op jit(solution)/shard_map/ppermute | solution.py:375
  59.5 3.2 %collective-permute-start.23 = (bf16[64,512]{1,0:T(8,128)(2,1)S(1)}, bf16[64,512]{1,0:T(8,128)(2,1)S(1)}, u32[]{:S(2)}, u32[]{:S(2)}) collective-permute-start(bf16[64,512]{1,0:T(8,128)(2,1)S(1)} %pad_maximum_fusion.2), channel_id=1, source_target_pairs={{0,16},{2,18},{4,20},{6,22},{8,24},{10,26},{12,28},{14,30},{16,0},... | collective-permute-start | bytes 196616 | tf_op jit(solution)/shard_map/ppermute | solution.py:369
  63.9 2.9 %load_weights.1 = (bf16[1,2048,256]{2,1,0:T(8,128)(2,1)S(1)}, bf16[1,2048,256]{2,1,0:T(8,128)(2,1)S(1)}, bf16[1,2048,256]{2,1,0:T(8,128)(2,1)S(1)}, bf16[1,2048,...) custom-call(bf16[1,2048,256]{2,1,0:T(8,128)(2,1)} %refs_0_.5, ...), custom_call_target="tpu_custom_call" | custom-call | tf_op jit(solution)/shard_map/load_weights/pallas_call | solution.py:181
  66.8 1.9 %collective-permute-done.24 = bf16[64,512]{1,0:T(8,128)(2,1)S(1)} collective-permute-done((bf16[64,512]{1,0:T(8,128)(2,1)S(1)}, bf16[64,512]{1,0:T(8,128)(2,1)S(1)}, u32[]{:S(2)}, u32[]{:S(2)}) %collective-permute-start.24) | collective-permute-done | bytes 65568 | tf_op jit(solution)/shard_map/ppermute | solution.py:369
  69.5 2.2 %routed_experts.2.kept_ref = bf16[64,2048]{1,0:T(8,128)(2,1)S(1)} custom-call(s32[2]{0:T(128)S(1)} %get-tuple-element.94.refs_0_, bf16[64,2176]{1,0:T(8,128)(2,1)S(1)} %constant_dynamic-update-slice_fusion.13.refs_1_, bf16[1,2048]{1,0:T(2,128)(2,1)S(1)} %reshape.96.refs_2_, bf16[16,2048]{1,0:T(8,128)(2,1)S(1)} %bitcast.10, ...), custom_call_target="tpu_custom_call" | custom-call | tf_op jit(solution)/shard_map/routed_experts/pallas_call | solution.py:342
  72.0 3.7 %collective-permute-done.25.refs_1_ = bf16[64,2176]{1,0:T(8,128)(2,1)S(1)} collective-permute-done((bf16[64,2176]{1,0:T(8,128)(2,1)S(1)}, bf16[64,2176]{1,0:T(8,128)(2,1)S(1)}, u32[]{:S(2)}, u32[]{:S(2)}) %collective-permute-start.25) | collective-permute-done | bytes 278560 | tf_op jit(solution)/shard_map/ppermute | solution.py:369
  75.7 2.2 %routed_experts.3 = bf16[64,2048]{1,0:T(8,128)(2,1)S(1)} custom-call(s32[2]{0:T(128)S(1)} %get-tuple-element.94.refs_0_, bf16[64,2176]{1,0:T(8,128)(2,1)S(1)} %collective-permute-done.25.refs_1_, bf16[1,2048]{1,0:T(2,128)(2,1)S(1)} %reshape.96.refs_2_, bf16[16,2048]{1,0:T(8,128)(2,1)S(1)} %bitcast.11, bf16[1,2048,256]{2,1,0:T(8,128)(2,1)S(1)} %get-tuple-element.101.refs_4_, ...), custom_call_target="tpu_custom_call" | custom-call | tf_op jit(solution)/shard_map/routed_experts/pallas_call | solution.py:342
  79.0 5.4 %collective-permute-done.26.other_ref = bf16[64,2048]{1,0:T(8,128)(2,1)S(1)} collective-permute-done((bf16[64,2048]{1,0:T(8,128)(2,1)S(1)}, bf16[64,2048]{1,0:T(8,128)(2,1)S(1)}, u32[]{:S(2)}, u32[]{:S(2)}) %collective-permute-start.26) | collective-permute-done | bytes 262176 | tf_op jit(solution)/shard_map/ppermute | solution.py:369
  85.0 1.6 %collective-permute-start.27 = (bf16[64,1024]{1,0:T(8,128)(2,1)S(1)}, bf16[64,1024]{1,0:T(8,128)(2,1)S(1)}, u32[]{:S(2)}, u32[]{:S(2)}) collective-permute-start(bf16[64,1024]{1,0:T(8,128)(2,1)S(1)} %get-tuple-element.108), channel_id=1, source_target_pairs={{0,1},{1,0},{2,3},{3,2},{4,5},{5,4},{6,7},{7,6},{8,9},{9,8},{10,11... | collective-permute-start | bytes 393224 | tf_op jit(solution)/shard_map/ppermute | solution.py:375
  86.6 3.4 %collective-permute-done.27 = bf16[64,1024]{1,0:T(8,128)(2,1)S(1)} collective-permute-done((bf16[64,1024]{1,0:T(8,128)(2,1)S(1)}, bf16[64,1024]{1,0:T(8,128)(2,1)S(1)}, u32[]{:S(2)}, u32[]{:S(2)}) %collective-permute-start.27) | collective-permute-done | bytes 131104 | tf_op jit(solution)/shard_map/ppermute | solution.py:375
  91.2 3.3 %collective-permute-start.28 = (bf16[16,1024]{1,0:T(8,128)(2,1)S(1)}, bf16[16,1024]{1,0:T(8,128)(2,1)S(1)}, u32[]{:S(2)}, u32[]{:S(2)}) collective-permute-start(bf16[16,1024]{1,0:T(8,128)(2,1)S(1)} %get-tuple-element.115), channel_id=1, source_target_pairs={{0,8},{2,10},{4,12},{6,14},{8,0},{10,2},{12,4},{14,6},{16,24},{18,... | collective-permute-start | bytes 98312 | tf_op jit(solution)/shard_map/ppermute | solution.py:369
  (127 shorter events, 23.6 us)
Async XLA Ops:
  0.6 12.5 %collective-permute-start.3 = (bf16[128,512]{1,0:T(8,128)(2,1)}, bf16[128,512]{1,0:T(8,128)(2,1)S(1)}, u32[]{:S(2)}, u32[]{:S(2)}) collective-permute-start(bf16[128,512]{1,0:T(8,128)(2,1)} %refs_0_.2), channel_id=1, source_target_pairs={{0,4},{2,6},{4,0},{6,2},{8,12},{10,14},{12,8},{14,10},{16,20},{18,... | collective-permute-start | bytes 393224 | tf_op jit(solution)/shard_map/ppermute | solution.py:369
  3.7 9.5 %collective-permute-start.4 = (bf16[128,512]{1,0:T(8,128)(2,1)}, bf16[128,512]{1,0:T(8,128)(2,1)S(1)}, u32[]{:S(2)}, u32[]{:S(2)}) collective-permute-start(bf16[128,512]{1,0:T(8,128)(2,1)} %refs_0_.2), channel_id=1, source_target_pairs={{0,2},{2,0},{4,6},{6,4},{8,10},{10,8},{12,14},{14,12},{16,18},{18,... | collective-permute-start | bytes 393224 | tf_op jit(solution)/shard_map/ppermute | solution.py:369
  4.7 6.4 %collective-permute-start.2 = (bf16[16,512]{1,0:T(8,128)(2,1)S(1)}, bf16[16,512]{1,0:T(8,128)(2,1)S(1)}, u32[]{:S(2)}, u32[]{:S(2)}) collective-permute-start(bf16[16,512]{1,0:T(8,128)(2,1)S(1)} %get-tuple-element.134), channel_id=1, source_target_pairs={{0,24},{2,26},{4,28},{6,30},{8,16},{10,18},{12,20},{14,22},{16,8},... | collective-permute-start | bytes 49160 | tf_op jit(solution)/shard_map/ppermute | solution.py:369
  15.6 22.2 %collective-permute-start.9 = (bf16[1,2048,256]{2,1,0:T(8,128)(2,1)}, bf16[1,2048,256]{2,1,0:T(8,128)(2,1)S(1)}, u32[]{:S(2)}, u32[]{:S(2)}) collective-permute-start(bf16[1,2048,256]{2,1,0:T(8,128)(2,1)} %refs_0_.5), channel_id=1, source_target_pairs={{0,2},{2,0},{4,6},{6,4},{8,10},{10,8},{12,14},{14,12},{16,18},{18,... | collective-permute-start | bytes 3145736 | tf_op jit(solution)/shard_map/ppermute | solution.py:369
  15.9 22.1 %collective-permute-start.10 = (bf16[1,2048,256]{2,1,0:T(8,128)(2,1)}, bf16[1,2048,256]{2,1,0:T(8,128)(2,1)S(1)}, u32[]{:S(2)}, u32[]{:S(2)}) collective-permute-start(bf16[1,2048,256]{2,1,0:T(8,128)(2,1)} %refs_2_), channel_id=1, source_target_pairs={{0,2},{2,0},{4,6},{6,4},{8,10},{10,8},{12,14},{14,12},{16,18},{18,... | collective-permute-start | bytes 3145736 | tf_op jit(solution)/shard_map/ppermute | solution.py:369
  16.2 21.7 %collective-permute-start.11 = (bf16[1,256,2048]{2,1,0:T(8,128)(2,1)}, bf16[1,256,2048]{2,1,0:T(8,128)(2,1)S(1)}, u32[]{:S(2)}, u32[]{:S(2)}) collective-permute-start(bf16[1,256,2048]{2,1,0:T(8,128)(2,1)} %refs_4_.3), channel_id=1, source_target_pairs={{0,2},{2,0},{4,6},{6,4},{8,10},{10,8},{12,14},{14,12},{16,18},{18,... | collective-permute-start | bytes 3145736 | tf_op jit(solution)/shard_map/ppermute | solution.py:369
  16.4 5.5 %collective-permute-start.8 = (bf16[16,512]{1,0:T(8,128)(2,1)S(1)}, bf16[16,512]{1,0:T(8,128)(2,1)S(1)}, u32[]{:S(2)}, u32[]{:S(2)}) collective-permute-start(bf16[16,512]{1,0:T(8,128)(2,1)S(1)} %get-tuple-element.127), channel_id=1, source_target_pairs={{0,24},{2,26},{4,28},{6,30},{8,16},{10,18},{12,20},{14,22},{16,8},... | collective-permute-start | bytes 49160 | tf_op jit(solution)/shard_map/ppermute | solution.py:369
  23.6 7.8 %collective-permute-start.12 = (bf16[128,512]{1,0:T(8,128)(2,1)S(1)}, bf16[128,512]{1,0:T(8,128)(2,1)S(1)}, u32[]{:S(2)}, u32[]{:S(2)}) collective-permute-start(bf16[128,512]{1,0:T(8,128)(2,1)S(1)} %constant_dynamic-update-slice_fusion.refs_0_), channel_id=1, source_target_pairs={{0,4},{2,6},{4,0},{6,2},{8,12},{10,14},{12,8},{14,10},{16,20},{18,... | collective-permute-start | bytes 393224 | tf_op jit(solution)/shard_map/ppermute | solution.py:369
  25.7 5.8 %collective-permute-start.13 = (bf16[128,512]{1,0:T(8,128)(2,1)S(1)}, bf16[128,512]{1,0:T(8,128)(2,1)S(1)}, u32[]{:S(2)}, u32[]{:S(2)}) collective-permute-start(bf16[128,512]{1,0:T(8,128)(2,1)S(1)} %constant_dynamic-update-slice_fusion.refs_0_), channel_id=1, source_target_pairs={{0,2},{2,0},{4,6},{6,4},{8,10},{10,8},{12,14},{14,12},{16,18},{18,... | collective-permute-start | bytes 393224 | tf_op jit(solution)/shard_map/ppermute | solution.py:369
  31.4 5.7 %collective-permute-start.18 = (bf16[128,512]{1,0:T(8,128)(2,1)S(1)}, bf16[128,512]{1,0:T(8,128)(2,1)S(1)}, u32[]{:S(2)}, u32[]{:S(2)}) collective-permute-start(bf16[128,512]{1,0:T(8,128)(2,1)S(1)} %copy-done.4), channel_id=1, source_target_pairs={{0,4},{2,6},{4,0},{6,2},{8,12},{10,14},{12,8},{14,10},{16,20},{18,... | collective-permute-start | bytes 393224 | tf_op jit(solution)/shard_map/ppermute | solution.py:369
  31.5 5.7 %collective-permute-start.14 = (bf16[128,512]{1,0:T(8,128)(2,1)S(1)}, bf16[128,512]{1,0:T(8,128)(2,1)S(1)}, u32[]{:S(2)}, u32[]{:S(2)}) collective-permute-start(bf16[128,512]{1,0:T(8,128)(2,1)S(1)} %collective-permute-done.12.refs_1_), channel_id=1, source_target_pairs={{0,2},{2,0},{4,6},{6,4},{8,10},{10,8},{12,14},{14,12},{16,18},{18,... | collective-permute-start | bytes 393224 | tf_op jit(solution)/shard_map/ppermute | solution.py:369
  37.1 13.9 %collective-permute-start.19 = (bf16[128,512]{1,0:T(8,128)(2,1)S(1)}, bf16[128,512]{1,0:T(8,128)(2,1)S(1)}, u32[]{:S(2)}, u32[]{:S(2)}) collective-permute-start(bf16[128,512]{1,0:T(8,128)(2,1)S(1)} %copy-done.4), channel_id=1, source_target_pairs={{0,2},{2,0},{4,6},{6,4},{8,10},{10,8},{12,14},{14,12},{16,18},{18,... | collective-permute-start | bytes 393224 | tf_op jit(solution)/shard_map/ppermute | solution.py:369
  37.1 13.9 %collective-permute-start.20 = (bf16[128,512]{1,0:T(8,128)(2,1)S(1)}, bf16[128,512]{1,0:T(8,128)(2,1)S(1)}, u32[]{:S(2)}, u32[]{:S(2)}) collective-permute-start(bf16[128,512]{1,0:T(8,128)(2,1)S(1)} %collective-permute-done.18.refs_5_), channel_id=1, source_target_pairs={{0,2},{2,0},{4,6},{6,4},{8,10},{10,8},{12,14},{14,12},{16,18},{18,... | collective-permute-start | bytes 393224 | tf_op jit(solution)/shard_map/ppermute | solution.py:369
  46.7 5.4 %collective-permute-start.16 = (bf16[16,1280]{1,0:T(8,128)(2,1)S(1)}, bf16[16,1280]{1,0:T(8,128)(2,1)S(1)}, u32[]{:S(2)}, u32[]{:S(2)}) collective-permute-start(bf16[16,1280]{1,0:T(8,128)(2,1)S(1)} %get-tuple-element.138), channel_id=1, source_target_pairs={{0,16},{2,18},{4,20},{6,22},{8,24},{10,26},{12,28},{14,30},{16,0},... | collective-permute-start | bytes 122888 | tf_op jit(solution)/shard_map/ppermute | solution.py:369
  48.4 5.8 %collective-permute-start.17 = (bf16[16,1280]{1,0:T(8,128)(2,1)S(1)}, bf16[16,1280]{1,0:T(8,128)(2,1)S(1)}, u32[]{:S(2)}, u32[]{:S(2)}) collective-permute-start(bf16[16,1280]{1,0:T(8,128)(2,1)S(1)} %get-tuple-element.137), channel_id=1, source_target_pairs={{0,24},{2,26},{4,28},{6,30},{8,16},{10,18},{12,20},{14,22},{16,8},... | collective-permute-start | bytes 122888 | tf_op jit(solution)/shard_map/ppermute | solution.py:369
  59.4 7.3 %collective-permute-start.22 = (bf16[64,512]{1,0:T(8,128)(2,1)S(1)}, bf16[64,512]{1,0:T(8,128)(2,1)S(1)}, u32[]{:S(2)}, u32[]{:S(2)}) collective-permute-start(bf16[64,512]{1,0:T(8,128)(2,1)S(1)} %pad_maximum_fusion.2), channel_id=1, source_target_pairs={{0,8},{2,10},{4,12},{6,14},{8,0},{10,2},{12,4},{14,6},{16,24},{18,... | collective-permute-start | bytes 196616 | tf_op jit(solution)/shard_map/ppermute | solution.py:369
  59.5 7.3 %collective-permute-start.23 = (bf16[64,512]{1,0:T(8,128)(2,1)S(1)}, bf16[64,512]{1,0:T(8,128)(2,1)S(1)}, u32[]{:S(2)}, u32[]{:S(2)}) collective-permute-start(bf16[64,512]{1,0:T(8,128)(2,1)S(1)} %pad_maximum_fusion.2), channel_id=1, source_target_pairs={{0,16},{2,18},{4,20},{6,22},{8,24},{10,26},{12,28},{14,30},{16,0},... | collective-permute-start | bytes 196616 | tf_op jit(solution)/shard_map/ppermute | solution.py:369
  62.7 6.1 %collective-permute-start.24 = (bf16[64,512]{1,0:T(8,128)(2,1)S(1)}, bf16[64,512]{1,0:T(8,128)(2,1)S(1)}, u32[]{:S(2)}, u32[]{:S(2)}) collective-permute-start(bf16[64,512]{1,0:T(8,128)(2,1)S(1)} %pad_maximum_fusion.2), channel_id=1, source_target_pairs={{0,24},{2,26},{4,28},{6,30},{8,16},{10,18},{12,20},{14,22},{16,8},... | collective-permute-start | bytes 196616 | tf_op jit(solution)/shard_map/ppermute | solution.py:369
  68.9 6.7 %collective-permute-start.25 = (bf16[64,2176]{1,0:T(8,128)(2,1)S(1)}, bf16[64,2176]{1,0:T(8,128)(2,1)S(1)}, u32[]{:S(2)}, u32[]{:S(2)}) collective-permute-start(bf16[64,2176]{1,0:T(8,128)(2,1)S(1)} %constant_dynamic-update-slice_fusion.13.refs_1_), channel_id=1, source_target_pairs={{0,4},{2,6},{4,0},{6,2},{8,12},{10,14},{12,8},{14,10},{16,20},{18,... | collective-permute-start | bytes 835592 | tf_op jit(solution)/shard_map/ppermute | solution.py:369
  77.9 6.4 %collective-permute-start.26 = (bf16[64,2048]{1,0:T(8,128)(2,1)S(1)}, bf16[64,2048]{1,0:T(8,128)(2,1)S(1)}, u32[]{:S(2)}, u32[]{:S(2)}) collective-permute-start(bf16[64,2048]{1,0:T(8,128)(2,1)S(1)} %routed_experts.3), channel_id=1, source_target_pairs={{0,4},{2,6},{4,0},{6,2},{8,12},{10,14},{12,8},{14,10},{16,20},{18,... | collective-permute-start | bytes 786440 | tf_op jit(solution)/shard_map/ppermute | solution.py:369
  85.0 5.0 %collective-permute-start.27 = (bf16[64,1024]{1,0:T(8,128)(2,1)S(1)}, bf16[64,1024]{1,0:T(8,128)(2,1)S(1)}, u32[]{:S(2)}, u32[]{:S(2)}) collective-permute-start(bf16[64,1024]{1,0:T(8,128)(2,1)S(1)} %get-tuple-element.108), channel_id=1, source_target_pairs={{0,1},{1,0},{2,3},{3,2},{4,5},{5,4},{6,7},{7,6},{8,9},{9,8},{10,11... | collective-permute-start | bytes 393224 | tf_op jit(solution)/shard_map/ppermute | solution.py:375
  90.0 5.8 %collective-permute-start.30 = (bf16[16,1024]{1,0:T(8,128)(2,1)S(1)}, bf16[16,1024]{1,0:T(8,128)(2,1)S(1)}, u32[]{:S(2)}, u32[]{:S(2)}) collective-permute-start(bf16[16,1024]{1,0:T(8,128)(2,1)S(1)} %get-tuple-element.116), channel_id=1, source_target_pairs={{0,24},{2,26},{4,28},{6,30},{8,16},{10,18},{12,20},{14,22},{16,8},... | collective-permute-start | bytes 98312 | tf_op jit(solution)/shard_map/ppermute | solution.py:369
  91.2 5.4 %collective-permute-start.29 = (bf16[16,1024]{1,0:T(8,128)(2,1)S(1)}, bf16[16,1024]{1,0:T(8,128)(2,1)S(1)}, u32[]{:S(2)}, u32[]{:S(2)}) collective-permute-start(bf16[16,1024]{1,0:T(8,128)(2,1)S(1)} %get-tuple-element.117), channel_id=1, source_target_pairs={{0,16},{2,18},{4,20},{6,22},{8,24},{10,26},{12,28},{14,30},{16,0},... | collective-permute-start | bytes 98312 | tf_op jit(solution)/shard_map/ppermute | solution.py:369
  91.2 5.5 %collective-permute-start.28 = (bf16[16,1024]{1,0:T(8,128)(2,1)S(1)}, bf16[16,1024]{1,0:T(8,128)(2,1)S(1)}, u32[]{:S(2)}, u32[]{:S(2)}) collective-permute-start(bf16[16,1024]{1,0:T(8,128)(2,1)S(1)} %get-tuple-element.115), channel_id=1, source_target_pairs={{0,8},{2,10},{4,12},{6,14},{8,0},{10,2},{12,4},{14,6},{16,24},{18,... | collective-permute-start | bytes 98312 | tf_op jit(solution)/shard_map/ppermute | solution.py:369
  (20 other events, 234.7 us)
where the time goes:
time: 97.9 us; the launch traced here: 97.4 us
  waiting for transfers between devices  35.5 us (36%)
  starting transfers between devices  29 us (30%)
  Pallas kernels  20.8 us (21%)
  local copies, waits for them, and re-layouts  6.83 us (7%)
  other arithmetic  3.12 us (3%)
  between operations  1.21 us (1%)
  matrix products  1.06 us (1%)
    ppermute x29, waiting for transfers between devices, swap(): return lax.ppermute(value, 'ep', [(i, i ^ mask) for i in range(n_ep)])  29.2 us
    ppermute x29, starting transfers between devices, swap(): return lax.ppermute(value, 'ep', [(i, i ^ mask) for i in range(n_ep)])  25.8 us
    pallas_call x1, Pallas kernels, attend(): pl.pallas_call(kernel, out_shape=jax.ShapeDtypeStruct((seq_count, width +...  8.57 us
    ppermute x2, waiting for transfers between devices, tp_swap(): return lax.ppermute(value, 'tp', [(i, (i + 1) % n_tp) for i in range(n_tp)])  6.24 us
    pallas_call x2, Pallas kernels, run_experts(): pl.pallas_call(kernel, out_shape=jax.ShapeDtypeStruct(shape, bf16), grid_...  4.44 us
    pallas_call x1, Pallas kernels, load(): pl.pallas_call(kernel, out_shape=pltpu.VMEM(shape, bf16), in_specs=[pl.Bl...  3.59 us
    ppermute x2, starting transfers between devices, tp_swap(): return lax.ppermute(value, 'tp', [(i, (i + 1) % n_tp) for i in range(n_tp)])  3.17 us
    pallas_call x1, Pallas kernels, load_weights(): pl.pallas_call(kernel, out_shape=tuple((pltpu.VMEM(w.shape, w.dtype) for...  2.85 us
  transfers between devices with their start and end apart: 31, of which 16 were waited for; matrix products, arithmetic and copies ran while one was open for 8% of the time, Pallas kernels for 18%

commit v1 on v0

v1 whole, which is shorter than its diff:
```python
import jax
import jax.numpy as jnp
from jax import lax
from jax.experimental import pallas as pl
from jax.experimental.pallas import tpu as pltpu
from jax.sharding import PartitionSpec as P


epsilon = 1e-06
routed_scale = 2.5
LANES = 128
bf16 = jnp.bfloat16
f32 = jnp.float32


def dot(a, b, dims=((1,), (0,)), precision=None):
    return lax.dot_general(a, b, (dims, ((), ())), precision=precision, preferred_element_type=f32)


def split3(value):
    high = value.astype(bf16)
    rest = value - high.astype(f32)
    mid = rest.astype(bf16)
    low = (rest - mid.astype(f32)).astype(bf16)
    return high, mid, low


def split2(value):
    high = value.astype(bf16)
    return high, (value - high.astype(f32)).astype(bf16)


def attend_kernel(
    lengths, q_ref, k_hbm, v_hbm, off_ref, gain_ref, mask_ref, out_ref, k_ref, v_ref, heads_ref, sems,
    *, seqs, heads, key_heads
):
    count, rows, head_size = k_ref.shape
    half = rows // 2
    positions = rows // key_heads
    block = LANES * key_heads
    group = heads // key_heads
    both = 2 * heads
    blocks = half // LANES
    off_blocks = positions // 2 // LANES

    def key_copy(s):
        live = pl.multiple_of((lengths[s] * key_heads + LANES - 1) // LANES * LANES, LANES)
        window = pl.ds(0, live)
        return pltpu.make_async_copy(k_hbm.at[s, window], k_ref.at[s, window], sems.at[0, s])

    def value_copy(s):
        return pltpu.make_async_copy(v_hbm.at[s], v_ref.at[s], sems.at[1, s])

    for first in range(0, count, seqs):
        for s in range(first, first + seqs):
            key_copy(s).start()
        for s in range(first, first + seqs):
            value_copy(s).start()

    row = lax.broadcasted_iota(jnp.int32, (both, half), 0)
    col = lax.broadcasted_iota(jnp.int32, (both, half), 1)
    place = jnp.where(row >= heads, positions // 2, 0) + col // key_heads
    mine = (col % key_heads) == ((row % heads) // group)
    place = jnp.where(mine, place, positions)
    low_row = row < heads
    scale = head_size ** (-0.5)
    spread = (
        lax.broadcasted_iota(jnp.int32, (LANES, block), 1) // key_heads
        == lax.broadcasted_iota(jnp.int32, (LANES, block), 0)
    ).astype(bf16)
    tri_row = lax.broadcasted_iota(jnp.int32, (LANES, 2 * LANES), 0)
    tri_col = lax.broadcasted_iota(jnp.int32, (LANES, 2 * LANES), 1)
    tri = ((tri_row > tri_col) | (tri_col >= LANES)).astype(bf16)
    top_row = lax.broadcasted_iota(jnp.int32, (both, LANES), 0) < heads

    for first in range(0, count, seqs):
        members = range(first, first + seqs)
        for s in members:
            key_copy(s).wait()
        scores = []
        for s in members:
            own = q_ref[s : s + 1, :]
            q8 = jnp.concatenate(
                [own[:, h * head_size : (h + 1) * head_size] for h in range(heads)] * 2, axis=0
            ).astype(bf16)
            s_lo = dot(q8, k_ref[s, :half, :], ((1,), (1,)))
            s_hi = dot(q8, k_ref[s, half:, :], ((1,), (1,)))
            scores.append(jnp.where(low_row, s_lo, s_hi) * scale)
        stacked = []
        for s in members:
            off = off_ref[s]
            off8 = jnp.concatenate([off[:, : positions // 2], off[:, positions // 2 :]], axis=0)
            stacked += [off8[:, b * LANES : (b + 1) * LANES] for b in range(off_blocks)]
        high, low = split2(jnp.concatenate(stacked, axis=0))
        wide = dot(high, spread) + dot(low, spread)
        keep_rows, valids, stops = [], [], []
        for i, s in enumerate(members):
            start = i * off_blocks
            offsets = jnp.concatenate(
                [wide[(start + b) * both : (start + b + 1) * both] for b in range(off_blocks)], axis=1
            )
            logits = scores[i] + offsets
            valid = place < lengths[s]
            tail = jnp.log(1.0 + jnp.exp(-jnp.abs(logits)))
            stops.append(jnp.minimum(logits, 0.0) - tail)
            keep = jnp.where(valid, -jnp.maximum(logits, 0.0) - tail, 0.0)
            keep_rows += [keep[:, b * LANES : (b + 1) * LANES] for b in range(blocks)]
            valids.append(valid)
        high, low = split2(jnp.concatenate(keep_rows, axis=0))
        sums = dot(high, tri) + dot(low, tri)
        sticks = []
        for i in range(seqs):
            after = [None] * blocks
            running = jnp.zeros((both, LANES), f32)
            for b in reversed(range(blocks)):
                base = (i * blocks + b) * both
                after[b] = sums[base : base + both, :LANES] + running
                running = running + sums[base : base + both, LANES:]
            upper = jnp.where(top_row, pltpu.roll(running, heads, 0), 0.0)
            after_sum = jnp.concatenate([a + upper for a in after], axis=1)
            sticks.append(jnp.where(valids[i], jnp.exp(stops[i] + after_sum), 0.0).astype(bf16))
        for s in members:
            value_copy(s).wait()
        for i, s in enumerate(members):
            o_lo = dot(sticks[i], v_ref[s, :half, :])
            o_hi = dot(sticks[i], v_ref[s, half:, :])
            out = o_lo + pltpu.roll(o_hi, heads, 0)
            for h in range(heads):
                heads_ref[s : s + 1, h * head_size : (h + 1) * head_size] = out[h : h + 1]

    values = heads_ref[...]
    width = values.shape[1]
    out_ref[:, :width] = (values * gain_ref[...].astype(f32)).astype(bf16)
    square = jnp.sum(values * values, axis=1, keepdims=True)
    first, second, third = [p.astype(f32) for p in split3(square)]
    lane = lax.broadcasted_iota(jnp.int32, (values.shape[0], LANES), 1)
    extra = jnp.where(lane == 0, first, jnp.where(lane == 1, second, jnp.where(lane == 2, third, 0.0)))
    out_ref[:, width : width + LANES] = extra.astype(bf16)
    out_ref[:, width + LANES :] = mask_ref[...]


def load_weights(weights):
    def kernel(*refs):
        count = len(weights)
        sources, targets, sems = refs[:count], refs[count : 2 * count], refs[-1]
        copies = [pltpu.make_async_copy(a, b, sems.at[i]) for i, (a, b) in enumerate(zip(sources, targets))]
        for copy in copies:
            copy.start()
        for copy in copies:
            copy.wait()

    return pl.pallas_call(
        kernel,
        out_shape=tuple(pltpu.VMEM(w.shape, w.dtype) for w in weights),
        in_specs=[pl.BlockSpec(memory_space=pltpu.HBM)] * len(weights),
        out_specs=tuple(pl.BlockSpec(memory_space=pltpu.VMEM) for _ in weights),
        scratch_shapes=[pltpu.SemaphoreType.DMA((len(weights),))],
        compiler_params=pltpu.CompilerParams(vmem_limit_bytes=4 * 1024 * 1024),
        name="load_weights",
    )(*[pltpu.with_memory_space_constraint(w, pltpu.HBM) for w in weights])


def attend(queries, key_cache, value_cache, offsets, lengths, gain_row, mask):
    seq_count, positions, key_heads, head_size = key_cache.shape
    heads = offsets.shape[1]
    rows = positions * key_heads
    shape = (seq_count, rows, head_size)
    width = heads * head_size
    total = width + LANES + mask.shape[1]
    hbm = pl.BlockSpec(memory_space=pltpu.HBM)

    def kernel(*refs):
        attend_kernel(*refs, seqs=8, heads=heads, key_heads=key_heads)

    return pl.pallas_call(
        kernel,
        out_shape=jax.ShapeDtypeStruct((seq_count, total), bf16),
        grid_spec=pltpu.PrefetchScalarGridSpec(
            num_scalar_prefetch=1,
            grid=(1,),
            in_specs=[whole((seq_count, width)), hbm, hbm, whole(offsets.shape), whole((1, width)), whole(mask.shape)],
            out_specs=whole((seq_count, total)),
            scratch_shapes=[
                pltpu.VMEM(shape, bf16),
                pltpu.VMEM(shape, bf16),
                pltpu.VMEM((seq_count, width), f32),
                pltpu.SemaphoreType.DMA((2, seq_count)),
            ],
        ),
        compiler_params=pltpu.CompilerParams(vmem_limit_bytes=24 * 1024 * 1024),
        cost_estimate=pl.CostEstimate(flops=2 * 10**9, transcendentals=10**6, bytes_accessed=2 * 10**7),
        name="stick_attend",
    )(
        lengths,
        queries,
        pltpu.with_memory_space_constraint(key_cache.reshape(shape), pltpu.HBM),
        pltpu.with_memory_space_constraint(value_cache.reshape(shape), pltpu.HBM),
        pltpu.with_memory_space_constraint(offsets, pltpu.VMEM),
        gain_row,
        mask,
    )


def pack(arrays, other):
    widths = [a.shape[1] for a in arrays]
    shape = (arrays[0].shape[0], sum(widths))

    def kernel(*refs):
        out_ref, second_ref, sems = refs[-3:]
        copies = [pltpu.make_async_copy(refs[-4], second_ref, sems.at[len(arrays)])]
        for i, ref in enumerate(refs[:-4]):
            window = pl.ds(sum(widths[:i]), widths[i])
            copies.append(pltpu.make_async_copy(ref, out_ref.at[:, window], sems.at[i]))
        for copy in copies:
            copy.start()
        for copy in copies:
            copy.wait()

    return pl.pallas_call(
        kernel,
        out_shape=(pltpu.VMEM(shape, bf16), pltpu.VMEM(other.shape, other.dtype)),
        in_specs=[pl.BlockSpec(memory_space=pltpu.HBM)] * (len(arrays) + 1),
        out_specs=(pl.BlockSpec(memory_space=pltpu.VMEM), pl.BlockSpec(memory_space=pltpu.VMEM)),
        scratch_shapes=[pltpu.SemaphoreType.DMA((len(arrays) + 1,))],
        compiler_params=pltpu.CompilerParams(vmem_limit_bytes=4 * 1024 * 1024),
        name="pack",
    )(*[pltpu.with_memory_space_constraint(a, pltpu.HBM) for a in (*arrays, other)])


def whole(shape):
    return pl.BlockSpec(shape, lambda *_: tuple(0 for _ in shape))


def project(rows, weights, skip=0):
    block, width = weights[0].shape
    shape = (rows.shape[0], width - skip)

    def kernel(rows_ref, *refs):
        total = None
        for i, weight in enumerate(refs[:-1]):
            piece = dot(rows_ref[:, i * block : (i + 1) * block], weight[:, skip:])
            total = piece if total is None else total + piece
        refs[-1][...] = total.astype(bf16)

    return pl.pallas_call(
        kernel,
        out_shape=jax.ShapeDtypeStruct(shape, bf16),
        in_specs=[whole(rows.shape)] + [whole(w.shape) for w in weights],
        out_specs=whole(shape),
        grid=(1,),
        compiler_params=pltpu.CompilerParams(vmem_limit_bytes=8 * 1024 * 1024),
        name="project",
    )(rows, *weights)


def out_kernel(*refs, count, width, extra):
    messages, weights, out_ref = refs[:count], refs[count:-1], refs[-1]
    rows = jnp.concatenate([m[:, :width] for m in messages], axis=0)
    pieces = [dot(rows, weight[:, :width], ((1,), (1,))).astype(bf16) for weight in weights]
    pieces.append(jnp.concatenate([m[:, width : width + extra] for m in messages], axis=0))
    out_ref[...] = jnp.concatenate(pieces, axis=1)


def out_project(messages, weights, width, extra):
    rows = sum(m.shape[0] for m in messages)
    shape = (rows, sum(w.shape[0] for w in weights) + extra)

    def kernel(*refs):
        out_kernel(*refs, count=len(messages), width=width, extra=extra)

    return pl.pallas_call(
        kernel,
        out_shape=jax.ShapeDtypeStruct(shape, bf16),
        in_specs=[whole(m.shape) for m in messages] + [whole(w.shape) for w in weights],
        out_specs=whole(shape),
        grid=(1,),
        compiler_params=pltpu.CompilerParams(vmem_limit_bytes=8 * 1024 * 1024),
        name="out_project",
    )(*messages, *weights)


def experts_kernel(place, rows_ref, gain_ref, router_ref, *refs, model, experts, groups, cols, seqs):
    gates, ups, downs = refs[:groups], refs[groups : 2 * groups], refs[2 * groups : 3 * groups]
    shared = refs[3 * groups : -3]
    keep_ref, send_ref, total_ref = refs[-3:]
    data = rows_ref[:, :model].astype(f32)
    factor = lax.rsqrt(jnp.sum(data * data, axis=-1, keepdims=True) * (1.0 / model) + epsilon)
    normed = (data * factor * gain_ref[...].astype(f32)).astype(bf16)
    mask = rows_ref[:, model:].astype(f32)[:, :experts]
    prob = jax.nn.sigmoid(dot(normed, router_ref[...], ((1,), (1,)))) * mask
    weight = routed_scale * prob / jnp.sum(prob, axis=-1, keepdims=True)
    lane = lax.broadcasted_iota(jnp.int32, weight.shape, 1)
    total = None
    for g in range(groups):
        for e in range(gates[g].shape[0]):
            expert = place[g] * gates[g].shape[0] + e
            mine = jnp.sum(jnp.where(lane == expert, weight, 0.0), axis=-1, keepdims=True)
            gate = dot(normed, gates[g][e])
            up = dot(normed, ups[g][e])
            hidden = (gate / (1.0 + jnp.exp(-gate)) * up).astype(bf16)
            piece = dot(hidden, downs[g][e]) * mine
            total = piece if total is None else total + piece
    total_ref[...] = total
    if shared:
        gate = dot(normed[:seqs], shared[0][...])
        up = dot(normed[:seqs], shared[1][...])
        hidden = (gate / (1.0 + jnp.exp(-gate)) * up).astype(bf16)
        total_ref[:seqs] = total[:seqs] + dot(hidden, shared[2][...])
    for target, i in ((send_ref, 1), (keep_ref, 0)):
        window = pl.ds(pl.multiple_of(place[groups + i], LANES), cols)
        target[...] = total_ref[:, window].astype(target.dtype)


def run_experts(rows, gain, router, gates, ups, downs, place, cols, seqs, shared=()):
    count = rows.shape[0]
    model = gates[0].shape[1]

    def kernel(*refs):
        experts_kernel(*refs, model=model, experts=router.shape[0], groups=len(gates), cols=cols, seqs=seqs)

    return pl.pallas_call(
        kernel,
        out_shape=(jax.ShapeDtypeStruct((count, cols), f32), jax.ShapeDtypeStruct((count, cols), bf16)),
        grid_spec=pltpu.PrefetchScalarGridSpec(
            num_scalar_prefetch=1,
            grid=(1,),
            in_specs=[whole(rows.shape), whole((1, model)), whole(router.shape)]
            + [pl.BlockSpec(memory_space=pltpu.VMEM)] * (3 * len(gates) + len(shared)),
            out_specs=(whole((count, cols)), whole((count, cols))),
            scratch_shapes=[pltpu.VMEM((count, model), f32)],
        ),
        compiler_params=pltpu.CompilerParams(vmem_limit_bytes=12 * 1024 * 1024),
        name="routed_experts",
    )(
        place,
        rows,
        gain,
        router,
        *[pltpu.with_memory_space_constraint(w, pltpu.VMEM) for w in (*gates, *ups, *downs, *shared)],
    )


def make_body(n_ep, n_tp):
    inner = 1 << ((n_ep.bit_length() - 1) // 2)
    outer = n_ep // inner
    masks = [1 << i for i in reversed(range(inner.bit_length() - 1))]

    def swap(value, mask):
        return lax.ppermute(value, "ep", [(i, i ^ mask) for i in range(n_ep)])

    def outer_swap(value, k):
        return swap(value, k * inner)

    def outer_exchange(messages):
        got = {}
        for k in reversed(range(1, outer)):
            got[k] = outer_swap(messages[k], k)
        return [messages[0]] + [got[k] for k in range(1, outer)]

    def tp_swap(value):
        return lax.ppermute(value, "tp", [(i, (i + 1) % n_tp) for i in range(n_tp)])

    def gather(value, over):
        pieces, order = [value], [0]
        for m in over:
            more = []
            for piece in pieces:
                more.append(swap(piece, m))
            pieces = pieces + more
            order = order + [o ^ m for o in order]
        return pieces, order

    def reverse_bits(value):
        result, width = jnp.uint32(0), inner
        while width > 1:
            result = (result << 1) | (value & 1)
            value = value >> 1
            width = width // 2
        return result

    def cut(value, start, size):
        return lax.dynamic_slice(value, (jnp.uint32(0), start), (value.shape[0], size))

    def body(
        tokens,
        attn_gain,
        query_weight,
        key_weight,
        value_weight,
        out_weight,
        head_gain,
        past_keys,
        past_values,
        break_offset,
        cache_lengths,
        ffn_gain,
        router_weight,
        expert_routes,
        expert_gate,
        expert_up,
        expert_down,
        shared_gate,
        shared_up,
        shared_down,
    ):
        seqs, model = tokens.shape
        experts = router_weight.shape[1]
        block = query_weight.shape[0]
        plane = block * inner
        cols = model // n_tp
        key_cols = key_weight.shape[1]
        heads_width = out_weight.shape[1]
        pad = -experts % LANES

        me = lax.axis_index("ep").astype(jnp.uint32)
        my_tp = lax.axis_index("tp").astype(jnp.uint32)
        my_inner = me & (inner - 1)
        my_outer = me >> (inner.bit_length() - 1)
        marks = [my_outer ^ k for k in range(outer)]
        starts = [m * plane for m in marks]
        blocks_at = [(my_inner ^ o) * block for o in range(inner)]
        back_at = [reverse_bits(my_inner ^ o) * block for o in range(inner)]
        own_start, other_start = my_tp * cols, ((my_tp + 1) & (n_tp - 1)) * cols
        row_starts = [m * (outer * seqs) for m in marks]
        place = jnp.stack([me, me ^ 1, own_start, other_start]).astype(jnp.int32)
        held = (tokens, starts, row_starts, blocks_at, back_at, own_start, place)
        held = lax.optimization_barrier(held)
        tokens, starts, row_starts, blocks_at, back_at, own_start, place = held

        query_pieces, order = gather(query_weight, masks)
        got = outer_exchange([cut(tokens, start, plane) for start in starts])
        group_tokens = jnp.concatenate(got, axis=0)

        def by_order(value):
            return jnp.concatenate([cut(value, blocks_at[o], block) for o in order], axis=1)

        gain_plane = cut(attn_gain.reshape(1, model), starts[0], plane)
        ordered = by_order(group_tokens)
        gained = (ordered.astype(f32) * by_order(gain_plane).astype(f32)).astype(bf16)
        query_pieces[0] = load_weights([query_weight])[0]
        query_part = project(gained, query_pieces)
        lane = lax.broadcasted_iota(jnp.int32, (1, 1, experts + pad), 2)
        query_part, routes, gains, late_tokens, packs = lax.optimization_barrier(
            (query_part, expert_routes, (head_gain, ffn_gain), tokens, (out_weight, key_weight, value_weight))
        )
        query_got = outer_exchange([query_part[k * seqs : (k + 1) * seqs] for k in range(outer)])
        routed_mask = jnp.sum((routes[:, :, None] == lane).astype(f32), axis=1).astype(bf16)
        gain_row = gains[0].reshape(1, -1)
        ffn_row = gains[1].reshape(1, -1)
        wide_tokens = late_tokens.astype(f32)
        factor = lax.rsqrt(jnp.mean(wide_tokens * wide_tokens, axis=-1, keepdims=True) + epsilon)
        packed, offsets = pack(packs, break_offset)
        late_pieces, _ = gather(packed, masks[:-1])
        queries = (sum(part.astype(f32) for part in query_got) * factor).astype(bf16).astype(f32)

        held = lax.optimization_barrier((queries, expert_gate, expert_up, expert_down))
        queries, expert_gate, expert_up, expert_down = held
        gates, ups, downs = [[w, swap(w, 1)] for w in (expert_gate, expert_up, expert_down)]
        scaled = attend(
            queries, past_keys, past_values, offsets, cache_lengths, gain_row, routed_mask
        )
        held = lax.optimization_barrier((scaled, gates, ups, downs, late_pieces))
        scaled, gates, ups, downs, late_pieces = held
        late_pieces = late_pieces + [swap(p, masks[-1]) for p in late_pieces]
        arrived = outer_exchange([scaled] * outer)
        group_mask = jnp.concatenate([m[:, heads_width + LANES :] for m in arrived], axis=0)
        own_part = out_project(arrived, late_pieces, heads_width, LANES)
        own_part, *shared = lax.optimization_barrier((own_part, shared_gate, shared_up, shared_down))
        shared = load_weights(shared)
        other_part = tp_swap(own_part)
        both = own_part.astype(f32) + other_part.astype(f32)
        square_total = jnp.sum(both[:, plane:], axis=1, keepdims=True)
        attention = both[:, :plane] * lax.rsqrt(square_total / (heads_width * n_tp) + epsilon)
        residual_part = (ordered.astype(f32) + attention).astype(bf16)

        residual_plane = jnp.concatenate([cut(residual_part, back_at[o], block) for o in range(inner)], axis=1)
        held = lax.optimization_barrier((residual_plane, gates, ups, downs, gained, shared))
        residual_plane, gates, ups, downs, gained, shared = held
        held_weights = load_weights((*gates, *ups, *downs))
        gates, ups, downs = held_weights[:2], held_weights[2:4], held_weights[4:]
        peers = outer_exchange([residual_plane] * outer)
        stacked = []
        for k in range(outer):
            stacked += [peers[k][(j ^ k) * seqs : (j ^ k) * seqs + seqs] for j in range(outer)]
        stacked = jnp.concatenate(stacked, axis=0)
        group_rows = jnp.concatenate(
            [lax.dynamic_slice(stacked, (row_starts[p], jnp.uint32(0)), (outer * seqs, plane)) for p in range(outer)]
            + [group_mask],
            axis=1,
        )
        group_rows, gates, ups, downs = lax.optimization_barrier((group_rows, gates, ups, downs))
        row_pieces, _ = gather(group_rows, masks[:-1])

        rest_part = project(gained, late_pieces, heads_width)
        rest_got = outer_exchange([rest_part[k * seqs : (k + 1) * seqs] for k in range(outer)])
        fresh = (sum(part.astype(f32) for part in rest_got) * factor).astype(bf16)
        own_rows = group_rows[:seqs, :model]

        router = router_weight.T
        results = []
        for i, piece in enumerate(row_pieces):
            if i > 0:
                piece, results = lax.optimization_barrier((piece, results))
            extra = shared if i == 0 else ()
            results.append(run_experts(piece, ffn_row, router, gates, ups, downs, place, cols, seqs, extra))
        sums = []
        for pair in results:
            sums.append(pair[0] + tp_swap(pair[1]).astype(f32))
        for m in reversed(masks[:-1]):
            half = len(sums) // 2
            back = [swap(v.astype(bf16), m) for v in sums[half:]]
            sums = [a + b.astype(f32) for a, b in zip(sums[:half], back)]
        value = sums[0]
        value_out = value.astype(bf16)
        parts = outer_exchange([value_out[k * seqs : (k + 1) * seqs] for k in range(outer)])
        total = value[:seqs] + sum(part.astype(f32) for part in parts[1:])
        mixed = (cut(own_rows, own_start, cols).astype(f32) + total).astype(bf16)
        return mixed, fresh[:, :key_cols], fresh[:, key_cols:]

    return body


def solution(mesh):
    placed = (
        P("ep", None),
        P(),
        P("ep", "tp"),
        P("ep", "tp"),
        P("ep", "tp"),
        P("ep", "tp"),
        P("tp"),
        P("ep", None, "tp", None),
        P("ep", None, "tp", None),
        P("ep", "tp", None),
        P("ep"),
        P(),
        P(),
        P("ep", None),
        P("ep", None, "tp"),
        P("ep", None, "tp"),
        P("ep", "tp", None),
        P(None, "tp"),
        P(None, "tp"),
        P("tp", None),
    )
    n_ep = mesh.shape["ep"]
    step = make_body(n_ep, mesh.shape["tp"])

    return jax.shard_map(
        step,
        mesh=mesh,
        in_specs=placed,
        out_specs=(P("ep", "tp"), P("ep", "tp"), P("ep", "tp")),
        check_vma=False,
    )
```

time: 97.9 us -> 89 us (0.909)
  waiting for transfers between devices: 35.5 us -> 22.4 us
  starting transfers between devices: 29 us -> 37.6 us
  local copies, waits for them, and re-layouts: 6.83 us -> 4.18 us
  matrix products: 1.06 us -> 0 us
    ppermute x29, starting transfers between devices: 25.8 us -> 34 us  [swap(): return lax.ppermute(value, 'ep', [(i, i ^ mask) for i in range(n_ep)])]
    ppermute x29, waiting for transfers between devices: 29.2 us -> 21.2 us  [swap(): return lax.ppermute(value, 'ep', [(i, i ^ mask) for i in range(n_ep)])]
    ppermute x2 -> x3, waiting for transfers between devices: 6.24 us -> 1.15 us  [tp_swap(): return lax.ppermute(value, 'tp', [(i, (i + 1) % n_tp) for i in range(n_tp)])]
    pallas_call x7 -> x6, Pallas kernels: 17.6 us -> 14.3 us  [the longest x1 7.84 us: attend(): pl.pallas_call(kernel, out_shape=jax.ShapeDtypeStruct((seq_count, total),...]
    pallas_call x1 -> x3, Pallas kernels: 2.85 us -> 5.66 us  [load_weights(): pl.pallas_call(kernel, out_shape=tuple((pltpu.VMEM(w.shape, w.dtype) for...]
    unnamed x41 -> x26, local copies, waits for them, and re-layouts: 2.6 us -> 0.82 us
    dot_general x2 -> x0, matrix products: 1.06 us -> none  [dot(): lax.dot_general(a, b, (dims, ((), ())), precision=precision, preferred_el...]
    ppermute x2 -> x3, starting transfers between devices: 3.17 us -> 3.68 us  [tp_swap(): return lax.ppermute(value, 'tp', [(i, (i + 1) % n_tp) for i in range(n_tp)])]
  transfers between devices with their start and end apart: 31 -> 32, of which waited for: 16 -> 12; matrix products, arithmetic and copies ran while one was open for 8% -> 6% of each run, Pallas kernels for 18% -> 20%
where the time goes in v1:
time: 89 us; the launch traced here: 88.6 us
  starting transfers between devices  37.6 us (42%)
  waiting for transfers between devices  22.4 us (25%)
  Pallas kernels  20.3 us (23%)
  local copies, waits for them, and re-layouts  4.18 us (5%)
  other arithmetic  3 us (3%)
  between operations  1.16 us (1%)
    ppermute x29, starting transfers between devices, swap(): return lax.ppermute(value, 'ep', [(i, i ^ mask) for i in range(n_ep)])  34 us
    ppermute x29, waiting for transfers between devices, swap(): return lax.ppermute(value, 'ep', [(i, i ^ mask) for i in range(n_ep)])  21.2 us
    pallas_call x1, Pallas kernels, attend(): pl.pallas_call(kernel, out_shape=jax.ShapeDtypeStruct((seq_count, total),...  7.84 us
    pallas_call x3, Pallas kernels, load_weights(): pl.pallas_call(kernel, out_shape=tuple((pltpu.VMEM(w.shape, w.dtype) for...  5.66 us
    pallas_call x2, Pallas kernels, run_experts(): pl.pallas_call(kernel, out_shape=(jax.ShapeDtypeStruct((count, cols), f32...  5.02 us
    ppermute x3, starting transfers between devices, tp_swap(): return lax.ppermute(value, 'tp', [(i, (i + 1) % n_tp) for i in range(n_tp)])  3.68 us
  transfers between devices with their start and end apart: 32, of which 12 were waited for; matrix products, arithmetic and copies ran while one was open for 6% of the time, Pallas kernels for 20%

profile of v1, /device:TPU:0, one launch (start us, length us, event | category | flops | bytes accessed | tf_op | source)
XLA Modules:
  0.0 88.6 jit_solution(1534568241858516319)
XLA Ops:
  0.6 3.0 %collective-permute-start.3 = (bf16[128,512]{1,0:T(8,128)(2,1)}, bf16[128,512]{1,0:T(8,128)(2,1)S(1)}, u32[]{:S(2)}, u32[]{:S(2)}) collective-permute-start(bf16[128,512]{1,0:T(8,128)(2,1)} %refs_0_.2), channel_id=1, source_target_pairs={{0,4},{2,6},{4,0},{6,2},{8,12},{10,14},{12,8},{14,10},{16,20},{18,... | collective-permute-start | bytes 393224 | tf_op jit(solution)/shard_map/ppermute | solution.py:349
  4.6 1.6 %collective-permute-start = (bf16[16,512]{1,0:T(8,128)(2,1)S(1)}, bf16[16,512]{1,0:T(8,128)(2,1)S(1)}, u32[]{:S(2)}, u32[]{:S(2)}) collective-permute-start(bf16[16,512]{1,0:T(8,128)(2,1)S(1)} %get-tuple-element.185), channel_id=1, source_target_pairs={{0,8},{2,10},{4,12},{6,14},{8,0},{10,2},{12,4},{14,6},{16,24},{18,... | collective-permute-start | bytes 49160 | tf_op jit(solution)/shard_map/ppermute | solution.py:349
  6.3 2.6 %collective-permute-start.1 = (bf16[16,512]{1,0:T(8,128)(2,1)S(1)}, bf16[16,512]{1,0:T(8,128)(2,1)S(1)}, u32[]{:S(2)}, u32[]{:S(2)}) collective-permute-start(bf16[16,512]{1,0:T(8,128)(2,1)S(1)} %get-tuple-element.184), channel_id=1, source_target_pairs={{0,16},{2,18},{4,20},{6,22},{8,24},{10,26},{12,28},{14,30},{16,0},... | collective-permute-start | bytes 49160 | tf_op jit(solution)/shard_map/ppermute | solution.py:349
  11.0 3.4 %collective-permute-done.2 = bf16[16,512]{1,0:T(8,128)(2,1)S(1)} collective-permute-done((bf16[16,512]{1,0:T(8,128)(2,1)S(1)}, bf16[16,512]{1,0:T(8,128)(2,1)S(1)}, u32[]{:S(2)}, u32[]{:S(2)}) %collective-permute-start.2) | collective-permute-done | bytes 16416 | tf_op jit(solution)/shard_map/ppermute | solution.py:349
  14.7 1.3 %collective-permute-done.5.refs_3_ = bf16[128,512]{1,0:T(8,128)(2,1)S(1)} collective-permute-done((bf16[128,512]{1,0:T(8,128)(2,1)S(1)}, bf16[128,512]{1,0:T(8,128)(2,1)S(1)}, u32[]{:S(2)}, u32[]{:S(2)}) %collective-permute-start.5) | collective-permute-done | bytes 131104 | tf_op jit(solution)/shard_map/ppermute | solution.py:349
  17.0 3.6 %collective-permute-start.8 = (bf16[16,512]{1,0:T(8,128)(2,1)S(1)}, bf16[16,512]{1,0:T(8,128)(2,1)S(1)}, u32[]{:S(2)}, u32[]{:S(2)}) collective-permute-start(bf16[16,512]{1,0:T(8,128)(2,1)S(1)} %get-tuple-element.176), channel_id=1, source_target_pairs={{0,24},{2,26},{4,28},{6,30},{8,16},{10,18},{12,20},{14,22},{16,8},... | collective-permute-start | bytes 49160 | tf_op jit(solution)/shard_map/ppermute | solution.py:349
  27.0 7.8 %stick_attend.1.refs_0_ = bf16[16,768]{1,0:T(8,128)(2,1)S(1)} custom-call(s32[16]{0:T(128)S(1)} %copy-done.1, f32[16,512]{1,0:T(8,128)S(1)} %fusion.4.refs_1_, bf16[16,2048,128]{2,1,0:T(8,128)(2,1)} %bitcast.9, bf16[16,2048,128]{2,1,0:T(8,128)(2,1)} %bitcast.10, f32[16,4,1024]{2,1,0:T(4,128)S(1)} %get-tuple-element.98.refs_4_, ...), custom_call_target="tpu_custom_call" | custom-call | flops 2000000000 | bytes 20000000 | tf_op jit(solution)/shard_map/stick_attend/pallas_call | solution.py:175
  35.7 3.9 %collective-permute-start.14 = (bf16[16,768]{1,0:T(8,128)(2,1)S(1)}, bf16[16,768]{1,0:T(8,128)(2,1)S(1)}, u32[]{:S(2)}, u32[]{:S(2)}) collective-permute-start(bf16[16,768]{1,0:T(8,128)(2,1)S(1)} %stick_attend.1.refs_0_), channel_id=1, source_target_pairs={{0,16},{2,18},{4,20},{6,22},{8,24},{10,26},{12,28},{14,30},{16,0},... | collective-permute-start | bytes 73736 | tf_op jit(solution)/shard_map/ppermute | solution.py:349
  39.9 1.5 %collective-permute-done.14.refs_2_ = bf16[16,768]{1,0:T(8,128)(2,1)S(1)} collective-permute-done((bf16[16,768]{1,0:T(8,128)(2,1)S(1)}, bf16[16,768]{1,0:T(8,128)(2,1)S(1)}, u32[]{:S(2)}, u32[]{:S(2)}) %collective-permute-start.14) | collective-permute-done | bytes 24608 | tf_op jit(solution)/shard_map/ppermute | solution.py:349
  41.4 3.8 %collective-permute-done.15.refs_3_ = bf16[16,768]{1,0:T(8,128)(2,1)S(1)} collective-permute-done((bf16[16,768]{1,0:T(8,128)(2,1)S(1)}, bf16[16,768]{1,0:T(8,128)(2,1)S(1)}, u32[]{:S(2)}, u32[]{:S(2)}) %collective-permute-start.15) | collective-permute-done | bytes 24608 | tf_op jit(solution)/shard_map/ppermute | solution.py:349
  45.5 1.6 %collective-permute-start.18 = (bf16[64,640]{1,0:T(8,128)(2,1)S(1)}, bf16[64,640]{1,0:T(8,128)(2,1)S(1)}, u32[]{:S(2)}, u32[]{:S(2)}) collective-permute-start(bf16[64,640]{1,0:T(8,128)(2,1)S(1)} %out_project.1), channel_id=1, source_target_pairs={{0,1},{1,0},{2,3},{3,2},{4,5},{5,4},{6,7},{7,6},{8,9},{9,8},{10,11... | collective-permute-start | bytes 245768 | tf_op jit(solution)/shard_map/ppermute | solution.py:361
  47.1 1.9 %load_weights.4 = (bf16[2048,256]{1,0:T(8,128)(2,1)S(1)}, bf16[2048,256]{1,0:T(8,128)(2,1)S(1)}, bf16[256,2048]{1,0:T(8,128)(2,1)S(1)}) custom-call(bf16[2048,256]{1,0:T(8,128)(2,1)} %refs_0_.5, bf16[2048,256]{1,0:T(8,128)(2,1)} %refs_1_.1, bf16[256,2048]{1,0:T(8,128)(2,1)} %refs_2_.1), custom_call_target="tpu_custom_call" | custom-call | tf_op jit(solution)/shard_map/load_weights/pallas_call | solution.py:152
  51.3 3.5 %collective-permute-start.21 = (bf16[64,512]{1,0:T(8,128)(2,1)S(1)}, bf16[64,512]{1,0:T(8,128)(2,1)S(1)}, u32[]{:S(2)}, u32[]{:S(2)}) collective-permute-start(bf16[64,512]{1,0:T(8,128)(2,1)S(1)} %pad_maximum_fusion.2), channel_id=1, source_target_pairs={{0,24},{2,26},{4,28},{6,30},{8,16},{10,18},{12,20},{14,22},{16,8},... | collective-permute-start | bytes 196616 | tf_op jit(solution)/shard_map/ppermute | solution.py:349
  54.9 2.9 %load_weights.5 = (bf16[1,2048,256]{2,1,0:T(8,128)(2,1)S(1)}, bf16[1,2048,256]{2,1,0:T(8,128)(2,1)S(1)}, bf16[1,2048,256]{2,1,0:T(8,128)(2,1)S(1)}, bf16[1,2048,...) custom-call(bf16[1,2048,256]{2,1,0:T(8,128)(2,1)} %refs_0_.6, ...), custom_call_target="tpu_custom_call" | custom-call | tf_op jit(solution)/shard_map/load_weights/pallas_call | solution.py:152
  58.1 1.3 %collective-permute-start.22 = (bf16[64,2176]{1,0:T(8,128)(2,1)S(1)}, bf16[64,2176]{1,0:T(8,128)(2,1)S(1)}, u32[]{:S(2)}, u32[]{:S(2)}) collective-permute-start(bf16[64,2176]{1,0:T(8,128)(2,1)S(1)} %constant_dynamic-update-slice_fusion.11.refs_1_), channel_id=1, source_target_pairs={{0,4},{2,6},{4,0},{6,2},{8,12},{10,14},{12,8},{14,10},{16,20},{18,... | collective-permute-start | bytes 835592 | tf_op jit(solution)/shard_map/ppermute | solution.py:349
  59.6 2.8 %routed_experts.2 = (f32[64,1024]{1,0:T(8,128)S(1)}, bf16[64,1024]{1,0:T(8,128)(2,1)S(1)}) custom-call(s32[4]{0:T(128)S(1)} %add_convert_fusion.1.refs_0_, bf16[64,2176]{1,0:T(8,128)(2,1)S(1)} %constant_dynamic-update-slice_fusion.11.refs_1_, bf16[1,2048]{1,0:T(2,128)(2,1)S(1)} %reshape.86.refs_2_, bf16[16,2048]{1,0:T(8,128)(2,1)S(1)} %bitcast.7, ...), custom_call_target="tpu_custom_call" | custom-call | tf_op jit(solution)/shard_map/routed_experts/pallas_call | solution.py:321
  62.4 2.3 %collective-permute-done.22.refs_1_ = bf16[64,2176]{1,0:T(8,128)(2,1)S(1)} collective-permute-done((bf16[64,2176]{1,0:T(8,128)(2,1)S(1)}, bf16[64,2176]{1,0:T(8,128)(2,1)S(1)}, u32[]{:S(2)}, u32[]{:S(2)}) %collective-permute-start.22) | collective-permute-done | bytes 278560 | tf_op jit(solution)/shard_map/ppermute | solution.py:349
  64.7 2.2 %routed_experts.3 = (f32[64,1024]{1,0:T(8,128)S(1)}, bf16[64,1024]{1,0:T(8,128)(2,1)S(1)}) custom-call(s32[4]{0:T(128)S(1)} %add_convert_fusion.1.refs_0_, bf16[64,2176]{1,0:T(8,128)(2,1)S(1)} %collective-permute-done.22.refs_1_, bf16[1,2048]{1,0:T(2,128)(2,1)S(1)} %reshape.86.refs_2_, bf16[16,2048]{1,0:T(8,128)(2,1)S(1)} %bitcast.8, ...), custom_call_target="tpu_custom_call" | custom-call | tf_op jit(solution)/shard_map/routed_experts/pallas_call | solution.py:321
  66.9 1.6 %collective-permute-start.24 = (bf16[64,1024]{1,0:T(8,128)(2,1)S(1)}, bf16[64,1024]{1,0:T(8,128)(2,1)S(1)}, u32[]{:S(2)}, u32[]{:S(2)}) collective-permute-start(bf16[64,1024]{1,0:T(8,128)(2,1)S(1)} %get-tuple-element.161), channel_id=1, source_target_pairs={{0,1},{1,0},{2,3},{3,2},{4,5},{5,4},{6,7},{7,6},{8,9},{9,8},{10,11... | collective-permute-start | bytes 393224 | tf_op jit(solution)/shard_map/ppermute | solution.py:361
  68.5 3.6 %collective-permute-start.30 = (bf16[16,512]{1,0:T(8,128)(2,1)S(1)}, bf16[16,512]{1,0:T(8,128)(2,1)S(1)}, u32[]{:S(2)}, u32[]{:S(2)}) collective-permute-start(bf16[16,512]{1,0:T(8,128)(2,1)S(1)} %get-tuple-element.170), channel_id=1, source_target_pairs={{0,16},{2,18},{4,20},{6,22},{8,24},{10,26},{12,28},{14,30},{16,0},... | collective-permute-start | bytes 49160 | tf_op jit(solution)/shard_map/ppermute | solution.py:349
  73.5 1.3 %collective-permute-start.25 = (bf16[64,1024]{1,0:T(8,128)(2,1)S(1)}, bf16[64,1024]{1,0:T(8,128)(2,1)S(1)}, u32[]{:S(2)}, u32[]{:S(2)}) collective-permute-start(bf16[64,1024]{1,0:T(8,128)(2,1)S(1)} %add_convert_fusion), channel_id=1, source_target_pairs={{0,4},{2,6},{4,0},{6,2},{8,12},{10,14},{12,8},{14,10},{16,20},{18,... | collective-permute-start | bytes 393224 | tf_op jit(solution)/shard_map/ppermute | solution.py:349
  74.7 2.9 %collective-permute-done.31 = bf16[16,512]{1,0:T(8,128)(2,1)S(1)} collective-permute-done((bf16[16,512]{1,0:T(8,128)(2,1)S(1)}, bf16[16,512]{1,0:T(8,128)(2,1)S(1)}, u32[]{:S(2)}, u32[]{:S(2)}) %collective-permute-start.31) | collective-permute-done | bytes 16416 | tf_op jit(solution)/shard_map/ppermute | solution.py:349
  78.6 3.6 %collective-permute-start.27 = (bf16[16,1024]{1,0:T(8,128)(2,1)S(1)}, bf16[16,1024]{1,0:T(8,128)(2,1)S(1)}, u32[]{:S(2)}, u32[]{:S(2)}) collective-permute-start(bf16[16,1024]{1,0:T(8,128)(2,1)S(1)} %get-tuple-element.167), channel_id=1, source_target_pairs={{0,16},{2,18},{4,20},{6,22},{8,24},{10,26},{12,28},{14,30},{16,0},... | collective-permute-start | bytes 98312 | tf_op jit(solution)/shard_map/ppermute | solution.py:349
  84.1 3.8 %collective-permute-done.28 = bf16[16,1024]{1,0:T(8,128)(2,1)S(1)} collective-permute-done((bf16[16,1024]{1,0:T(8,128)(2,1)S(1)}, bf16[16,1024]{1,0:T(8,128)(2,1)S(1)}, u32[]{:S(2)}, u32[]{:S(2)}) %collective-permute-start.28) | collective-permute-done | bytes 32800 | tf_op jit(solution)/shard_map/ppermute | solution.py:349
  (110 shorter events, 19.5 us)
Async XLA Ops:
  0.6 13.9 %collective-permute-start.3 = (bf16[128,512]{1,0:T(8,128)(2,1)}, bf16[128,512]{1,0:T(8,128)(2,1)S(1)}, u32[]{:S(2)}, u32[]{:S(2)}) collective-permute-start(bf16[128,512]{1,0:T(8,128)(2,1)} %refs_0_.2), channel_id=1, source_target_pairs={{0,4},{2,6},{4,0},{6,2},{8,12},{10,14},{12,8},{14,10},{16,20},{18,... | collective-permute-start | bytes 393224 | tf_op jit(solution)/shard_map/ppermute | solution.py:349
  3.7 11.0 %collective-permute-start.4 = (bf16[128,512]{1,0:T(8,128)(2,1)}, bf16[128,512]{1,0:T(8,128)(2,1)S(1)}, u32[]{:S(2)}, u32[]{:S(2)}) collective-permute-start(bf16[128,512]{1,0:T(8,128)(2,1)} %refs_0_.2), channel_id=1, source_target_pairs={{0,2},{2,0},{4,6},{6,4},{8,10},{10,8},{12,14},{14,12},{16,18},{18,... | collective-permute-start | bytes 393224 | tf_op jit(solution)/shard_map/ppermute | solution.py:349
  4.6 6.3 %collective-permute-start = (bf16[16,512]{1,0:T(8,128)(2,1)S(1)}, bf16[16,512]{1,0:T(8,128)(2,1)S(1)}, u32[]{:S(2)}, u32[]{:S(2)}) collective-permute-start(bf16[16,512]{1,0:T(8,128)(2,1)S(1)} %get-tuple-element.185), channel_id=1, source_target_pairs={{0,8},{2,10},{4,12},{6,14},{8,0},{10,2},{12,4},{14,6},{16,24},{18,... | collective-permute-start | bytes 49160 | tf_op jit(solution)/shard_map/ppermute | solution.py:349
  8.9 5.5 %collective-permute-start.2 = (bf16[16,512]{1,0:T(8,128)(2,1)S(1)}, bf16[16,512]{1,0:T(8,128)(2,1)S(1)}, u32[]{:S(2)}, u32[]{:S(2)}) collective-permute-start(bf16[16,512]{1,0:T(8,128)(2,1)S(1)} %get-tuple-element.183), channel_id=1, source_target_pairs={{0,24},{2,26},{4,28},{6,30},{8,16},{10,18},{12,20},{14,22},{16,8},... | collective-permute-start | bytes 49160 | tf_op jit(solution)/shard_map/ppermute | solution.py:349
  16.2 5.4 %collective-permute-start.6 = (bf16[16,512]{1,0:T(8,128)(2,1)S(1)}, bf16[16,512]{1,0:T(8,128)(2,1)S(1)}, u32[]{:S(2)}, u32[]{:S(2)}) collective-permute-start(bf16[16,512]{1,0:T(8,128)(2,1)S(1)} %get-tuple-element.175), channel_id=1, source_target_pairs={{0,8},{2,10},{4,12},{6,14},{8,0},{10,2},{12,4},{14,6},{16,24},{18,... | collective-permute-start | bytes 49160 | tf_op jit(solution)/shard_map/ppermute | solution.py:349
  17.0 5.5 %collective-permute-start.8 = (bf16[16,512]{1,0:T(8,128)(2,1)S(1)}, bf16[16,512]{1,0:T(8,128)(2,1)S(1)}, u32[]{:S(2)}, u32[]{:S(2)}) collective-permute-start(bf16[16,512]{1,0:T(8,128)(2,1)S(1)} %get-tuple-element.176), channel_id=1, source_target_pairs={{0,24},{2,26},{4,28},{6,30},{8,16},{10,18},{12,20},{14,22},{16,8},... | collective-permute-start | bytes 49160 | tf_op jit(solution)/shard_map/ppermute | solution.py:349
  22.6 12.2 %collective-permute-start.10 = (bf16[1,2048,256]{2,1,0:T(8,128)(2,1)}, bf16[1,2048,256]{2,1,0:T(8,128)(2,1)S(1)}, u32[]{:S(2)}, u32[]{:S(2)}) collective-permute-start(bf16[1,2048,256]{2,1,0:T(8,128)(2,1)} %refs_2_.2), channel_id=1, source_target_pairs={{0,2},{2,0},{4,6},{6,4},{8,10},{10,8},{12,14},{14,12},{16,18},{18,... | collective-permute-start | bytes 3145736 | tf_op jit(solution)/shard_map/ppermute | solution.py:349
  22.7 12.2 %collective-permute-start.11 = (bf16[1,256,2048]{2,1,0:T(8,128)(2,1)}, bf16[1,256,2048]{2,1,0:T(8,128)(2,1)S(1)}, u32[]{:S(2)}, u32[]{:S(2)}) collective-permute-start(bf16[1,256,2048]{2,1,0:T(8,128)(2,1)} %refs_4_), channel_id=1, source_target_pairs={{0,2},{2,0},{4,6},{6,4},{8,10},{10,8},{12,14},{14,12},{16,18},{18,... | collective-permute-start | bytes 3145736 | tf_op jit(solution)/shard_map/ppermute | solution.py:349
  23.2 11.7 %collective-permute-start.9 = (bf16[1,2048,256]{2,1,0:T(8,128)(2,1)}, bf16[1,2048,256]{2,1,0:T(8,128)(2,1)S(1)}, u32[]{:S(2)}, u32[]{:S(2)}) collective-permute-start(bf16[1,2048,256]{2,1,0:T(8,128)(2,1)} %refs_0_.6), channel_id=1, source_target_pairs={{0,2},{2,0},{4,6},{6,4},{8,10},{10,8},{12,14},{14,12},{16,18},{18,... | collective-permute-start | bytes 3145736 | tf_op jit(solution)/shard_map/ppermute | solution.py:349
  24.3 10.5 %collective-permute-start.12 = (bf16[128,1024]{1,0:T(8,128)(2,1)S(1)}, bf16[128,1024]{1,0:T(8,128)(2,1)S(1)}, u32[]{:S(2)}, u32[]{:S(2)}) collective-permute-start(bf16[128,1024]{1,0:T(8,128)(2,1)S(1)} %get-tuple-element.106.refs_4_.refs_0_), channel_id=1, source_target_pairs={{0,4},{2,6},{4,0},{6,2},{8,12},{10,14},{12,8},{14,10},{16,20},{18,... | collective-permute-start | bytes 786440 | tf_op jit(solution)/shard_map/ppermute | solution.py:349
  34.9 10.3 %collective-permute-start.16 = (bf16[128,1024]{1,0:T(8,128)(2,1)S(1)}, bf16[128,1024]{1,0:T(8,128)(2,1)S(1)}, u32[]{:S(2)}, u32[]{:S(2)}) collective-permute-start(bf16[128,1024]{1,0:T(8,128)(2,1)S(1)} %get-tuple-element.106.refs_4_.refs_0_), channel_id=1, source_target_pairs={{0,2},{2,0},{4,6},{6,4},{8,10},{10,8},{12,14},{14,12},{16,18},{18,... | collective-permute-start | bytes 786440 | tf_op jit(solution)/shard_map/ppermute | solution.py:349
  35.0 10.2 %collective-permute-start.17 = (bf16[128,1024]{1,0:T(8,128)(2,1)S(1)}, bf16[128,1024]{1,0:T(8,128)(2,1)S(1)}, u32[]{:S(2)}, u32[]{:S(2)}) collective-permute-start(bf16[128,1024]{1,0:T(8,128)(2,1)S(1)} %collective-permute-done.12.refs_5_.refs_1_), channel_id=1, source_target_pairs={{0,2},{2,0},{4,6},{6,4},{8,10},{10,8},{12,14},{14,12},{16,18},{18,... | collective-permute-start | bytes 786440 | tf_op jit(solution)/shard_map/ppermute | solution.py:349
  35.7 5.7 %collective-permute-start.14 = (bf16[16,768]{1,0:T(8,128)(2,1)S(1)}, bf16[16,768]{1,0:T(8,128)(2,1)S(1)}, u32[]{:S(2)}, u32[]{:S(2)}) collective-permute-start(bf16[16,768]{1,0:T(8,128)(2,1)S(1)} %stick_attend.1.refs_0_), channel_id=1, source_target_pairs={{0,16},{2,18},{4,20},{6,22},{8,24},{10,26},{12,28},{14,30},{16,0},... | collective-permute-start | bytes 73736 | tf_op jit(solution)/shard_map/ppermute | solution.py:349
  39.6 5.6 %collective-permute-start.15 = (bf16[16,768]{1,0:T(8,128)(2,1)S(1)}, bf16[16,768]{1,0:T(8,128)(2,1)S(1)}, u32[]{:S(2)}, u32[]{:S(2)}) collective-permute-start(bf16[16,768]{1,0:T(8,128)(2,1)S(1)} %stick_attend.1.refs_0_), channel_id=1, source_target_pairs={{0,24},{2,26},{4,28},{6,30},{8,16},{10,18},{12,20},{14,22},{16,8},... | collective-permute-start | bytes 73736 | tf_op jit(solution)/shard_map/ppermute | solution.py:349
  50.4 7.3 %collective-permute-start.19 = (bf16[64,512]{1,0:T(8,128)(2,1)S(1)}, bf16[64,512]{1,0:T(8,128)(2,1)S(1)}, u32[]{:S(2)}, u32[]{:S(2)}) collective-permute-start(bf16[64,512]{1,0:T(8,128)(2,1)S(1)} %pad_maximum_fusion.2), channel_id=1, source_target_pairs={{0,8},{2,10},{4,12},{6,14},{8,0},{10,2},{12,4},{14,6},{16,24},{18,... | collective-permute-start | bytes 196616 | tf_op jit(solution)/shard_map/ppermute | solution.py:349
  50.5 7.3 %collective-permute-start.20 = (bf16[64,512]{1,0:T(8,128)(2,1)S(1)}, bf16[64,512]{1,0:T(8,128)(2,1)S(1)}, u32[]{:S(2)}, u32[]{:S(2)}) collective-permute-start(bf16[64,512]{1,0:T(8,128)(2,1)S(1)} %pad_maximum_fusion.2), channel_id=1, source_target_pairs={{0,16},{2,18},{4,20},{6,22},{8,24},{10,26},{12,28},{14,30},{16,0},... | collective-permute-start | bytes 196616 | tf_op jit(solution)/shard_map/ppermute | solution.py:349
  51.3 6.5 %collective-permute-start.21 = (bf16[64,512]{1,0:T(8,128)(2,1)S(1)}, bf16[64,512]{1,0:T(8,128)(2,1)S(1)}, u32[]{:S(2)}, u32[]{:S(2)}) collective-permute-start(bf16[64,512]{1,0:T(8,128)(2,1)S(1)} %pad_maximum_fusion.2), channel_id=1, source_target_pairs={{0,24},{2,26},{4,28},{6,30},{8,16},{10,18},{12,20},{14,22},{16,8},... | collective-permute-start | bytes 196616 | tf_op jit(solution)/shard_map/ppermute | solution.py:349
  58.1 6.6 %collective-permute-start.22 = (bf16[64,2176]{1,0:T(8,128)(2,1)S(1)}, bf16[64,2176]{1,0:T(8,128)(2,1)S(1)}, u32[]{:S(2)}, u32[]{:S(2)}) collective-permute-start(bf16[64,2176]{1,0:T(8,128)(2,1)S(1)} %constant_dynamic-update-slice_fusion.11.refs_1_), channel_id=1, source_target_pairs={{0,4},{2,6},{4,0},{6,2},{8,12},{10,14},{12,8},{14,10},{16,20},{18,... | collective-permute-start | bytes 835592 | tf_op jit(solution)/shard_map/ppermute | solution.py:349
  66.9 6.5 %collective-permute-start.24 = (bf16[64,1024]{1,0:T(8,128)(2,1)S(1)}, bf16[64,1024]{1,0:T(8,128)(2,1)S(1)}, u32[]{:S(2)}, u32[]{:S(2)}) collective-permute-start(bf16[64,1024]{1,0:T(8,128)(2,1)S(1)} %get-tuple-element.161), channel_id=1, source_target_pairs={{0,1},{1,0},{2,3},{3,2},{4,5},{5,4},{6,7},{7,6},{8,9},{9,8},{10,11... | collective-permute-start | bytes 393224 | tf_op jit(solution)/shard_map/ppermute | solution.py:361
  68.5 6.2 %collective-permute-start.29 = (bf16[16,512]{1,0:T(8,128)(2,1)S(1)}, bf16[16,512]{1,0:T(8,128)(2,1)S(1)}, u32[]{:S(2)}, u32[]{:S(2)}) collective-permute-start(bf16[16,512]{1,0:T(8,128)(2,1)S(1)} %get-tuple-element.168), channel_id=1, source_target_pairs={{0,8},{2,10},{4,12},{6,14},{8,0},{10,2},{12,4},{14,6},{16,24},{18,... | collective-permute-start | bytes 49160 | tf_op jit(solution)/shard_map/ppermute | solution.py:349
  68.5 6.2 %collective-permute-start.30 = (bf16[16,512]{1,0:T(8,128)(2,1)S(1)}, bf16[16,512]{1,0:T(8,128)(2,1)S(1)}, u32[]{:S(2)}, u32[]{:S(2)}) collective-permute-start(bf16[16,512]{1,0:T(8,128)(2,1)S(1)} %get-tuple-element.170), channel_id=1, source_target_pairs={{0,16},{2,18},{4,20},{6,22},{8,24},{10,26},{12,28},{14,30},{16,0},... | collective-permute-start | bytes 49160 | tf_op jit(solution)/shard_map/ppermute | solution.py:349
  72.1 5.5 %collective-permute-start.31 = (bf16[16,512]{1,0:T(8,128)(2,1)S(1)}, bf16[16,512]{1,0:T(8,128)(2,1)S(1)}, u32[]{:S(2)}, u32[]{:S(2)}) collective-permute-start(bf16[16,512]{1,0:T(8,128)(2,1)S(1)} %get-tuple-element.169), channel_id=1, source_target_pairs={{0,24},{2,26},{4,28},{6,30},{8,16},{10,18},{12,20},{14,22},{16,8},... | collective-permute-start | bytes 49160 | tf_op jit(solution)/shard_map/ppermute | solution.py:349
  78.6 5.5 %collective-permute-start.27 = (bf16[16,1024]{1,0:T(8,128)(2,1)S(1)}, bf16[16,1024]{1,0:T(8,128)(2,1)S(1)}, u32[]{:S(2)}, u32[]{:S(2)}) collective-permute-start(bf16[16,1024]{1,0:T(8,128)(2,1)S(1)} %get-tuple-element.167), channel_id=1, source_target_pairs={{0,16},{2,18},{4,20},{6,22},{8,24},{10,26},{12,28},{14,30},{16,0},... | collective-permute-start | bytes 98312 | tf_op jit(solution)/shard_map/ppermute | solution.py:349
  82.2 5.7 %collective-permute-start.28 = (bf16[16,1024]{1,0:T(8,128)(2,1)S(1)}, bf16[16,1024]{1,0:T(8,128)(2,1)S(1)}, u32[]{:S(2)}, u32[]{:S(2)}) collective-permute-start(bf16[16,1024]{1,0:T(8,128)(2,1)S(1)} %get-tuple-element.166), channel_id=1, source_target_pairs={{0,24},{2,26},{4,28},{6,30},{8,16},{10,18},{12,20},{14,22},{16,8},... | collective-permute-start | bytes 98312 | tf_op jit(solution)/shard_map/ppermute | solution.py:349
  (14 other events, 145.4 us)

commit v2 on v1

--- a/solution.py
+++ b/solution.py
@@ -130,7 +130,7 @@
 
     values = heads_ref[...]
     width = values.shape[1]
-    out_ref[:, :width] = (values * gain_ref[...].astype(f32)).astype(bf16)
+    out_ref[:, :width] = (values * gain_ref[...].astype(f32).reshape(1, width)).astype(bf16)
     square = jnp.sum(values * values, axis=1, keepdims=True)
     first, second, third = [p.astype(f32) for p in split3(square)]
     lane = lax.broadcasted_iota(jnp.int32, (values.shape[0], LANES), 1)
@@ -178,7 +178,7 @@
         grid_spec=pltpu.PrefetchScalarGridSpec(
             num_scalar_prefetch=1,
             grid=(1,),
-            in_specs=[whole((seq_count, width)), hbm, hbm, whole(offsets.shape), whole((1, width)), whole(mask.shape)],
+            in_specs=[whole((seq_count, width)), hbm, hbm, whole(offsets.shape), whole((width,)), whole(mask.shape)],
             out_specs=whole((seq_count, total)),
             scratch_shapes=[
                 pltpu.VMEM(shape, bf16),
@@ -191,40 +191,80 @@
         cost_estimate=pl.CostEstimate(flops=2 * 10**9, transcendentals=10**6, bytes_accessed=2 * 10**7),
         name="stick_attend",
     )(
-        lengths,
+        pltpu.with_memory_space_constraint(lengths, pltpu.VMEM),
         queries,
         pltpu.with_memory_space_constraint(key_cache.reshape(shape), pltpu.HBM),
         pltpu.with_memory_space_constraint(value_cache.reshape(shape), pltpu.HBM),
         pltpu.with_memory_space_constraint(offsets, pltpu.VMEM),
-        gain_row,
+        pltpu.with_memory_space_constraint(gain_row, pltpu.VMEM),
         mask,
     )
 
 
-def pack(arrays, other):
+def pack(arrays, others, tokens, routes, lanes):
     widths = [a.shape[1] for a in arrays]
     shape = (arrays[0].shape[0], sum(widths))
-
-    def kernel(*refs):
-        out_ref, second_ref, sems = refs[-3:]
-        copies = [pltpu.make_async_copy(refs[-4], second_ref, sems.at[len(arrays)])]
-        for i, ref in enumerate(refs[:-4]):
+    count = len(arrays)
+    seqs, model = tokens.shape
+    tops = routes.shape[0]
+
+    extra = len(others)
+
+    def kernel(tokens_hbm, routes_hbm, *refs):
+        other_refs, refs = refs[:extra], refs[extra:]
+        out_ref, factor_ref, mask_ref = refs[count : count + 3]
+        targets = refs[count + 3 : count + 3 + extra]
+        tokens_ref, routes_ref, sems = refs[count + 3 + extra :]
+        early = [
+            pltpu.make_async_copy(tokens_hbm, tokens_ref, sems.at[count + extra]),
+            pltpu.make_async_copy(routes_hbm, routes_ref, sems.at[count + extra + 1]),
+        ]
+        for copy in early:
+            copy.start()
+        copies = [
+            pltpu.make_async_copy(source, target, sems.at[count + i])
+            for i, (source, target) in enumerate(zip(other_refs, targets))
+        ]
+        for i, ref in enumerate(refs[:count]):
             window = pl.ds(sum(widths[:i]), widths[i])
             copies.append(pltpu.make_async_copy(ref, out_ref.at[:, window], sems.at[i]))
         for copy in copies:
             copy.start()
+        for copy in early:
+            copy.wait()
+        data = tokens_ref[...].astype(f32)
+        factor = lax.rsqrt(jnp.sum(data * data, axis=-1, keepdims=True) * (1.0 / model) + epsilon)
+        factor_ref[...] = jnp.broadcast_to(factor, factor_ref.shape)
+        slot = lax.broadcasted_iota(jnp.int32, (lanes, seqs), 0)
+        chosen = jnp.zeros((lanes, seqs), f32)
+        for i in range(tops):
+            chosen = chosen + jnp.where(routes_ref[i : i + 1, :] == slot, 1.0, 0.0)
+        eye = (
+            lax.broadcasted_iota(jnp.int32, (lanes, lanes), 0) == lax.broadcasted_iota(jnp.int32, (lanes, lanes), 1)
+        ).astype(bf16)
+        mask_ref[...] = dot(chosen.astype(bf16), eye, ((0,), (0,))).astype(bf16)
         for copy in copies:
             copy.wait()
 
+    hbm, vmem = pl.BlockSpec(memory_space=pltpu.HBM), pl.BlockSpec(memory_space=pltpu.VMEM)
     return pl.pallas_call(
         kernel,
-        out_shape=(pltpu.VMEM(shape, bf16), pltpu.VMEM(other.shape, other.dtype)),
-        in_specs=[pl.BlockSpec(memory_space=pltpu.HBM)] * (len(arrays) + 1),
-        out_specs=(pl.BlockSpec(memory_space=pltpu.VMEM), pl.BlockSpec(memory_space=pltpu.VMEM)),
-        scratch_shapes=[pltpu.SemaphoreType.DMA((len(arrays) + 1,))],
+        out_shape=(
+            pltpu.VMEM(shape, bf16),
+            pltpu.VMEM((seqs, LANES), f32),
+            pltpu.VMEM((seqs, lanes), bf16),
+            *[pltpu.VMEM(x.shape, x.dtype) for x in others],
+        ),
+        in_specs=[hbm] * (count + extra + 2),
+        out_specs=(vmem,) * (3 + extra),
+        scratch_shapes=[
+            pltpu.VMEM(tokens.shape, tokens.dtype),
+            pltpu.VMEM(routes.shape, routes.dtype),
+            pltpu.SemaphoreType.DMA((count + extra + 2,)),
+        ],
         compiler_params=pltpu.CompilerParams(vmem_limit_bytes=4 * 1024 * 1024),
         name="pack",
-    )(*[pltpu.with_memory_space_constraint(a, pltpu.HBM) for a in (*arrays, other)])
+    )(*[pltpu.with_memory_space_constraint(a, pltpu.HBM) for a in (tokens, routes, *others, *arrays)])
 
 
 def whole(shape):
@@ -439,25 +479,23 @@
         gained = (ordered.astype(f32) * by_order(gain_plane).astype(f32)).astype(bf16)
         query_pieces[0] = load_weights([query_weight])[0]
         query_part = project(gained, query_pieces)
-        lane = lax.broadcasted_iota(jnp.int32, (1, 1, experts + pad), 2)
         query_part, routes, gains, late_tokens, packs = lax.optimization_barrier(
             (query_part, expert_routes, (head_gain, ffn_gain), tokens, (out_weight, key_weight, value_weight))
         )
         query_got = outer_exchange([query_part[k * seqs : (k + 1) * seqs] for k in range(outer)])
-        routed_mask = jnp.sum((routes[:, :, None] == lane).astype(f32), axis=1).astype(bf16)
-        gain_row = gains[0].reshape(1, -1)
         ffn_row = gains[1].reshape(1, -1)
-        wide_tokens = late_tokens.astype(f32)
-        factor = lax.rsqrt(jnp.mean(wide_tokens * wide_tokens, axis=-1, keepdims=True) + epsilon)
-        packed, offsets = pack(packs, break_offset)
+        packed, factor, routed_mask, offsets, gain_row, lengths = pack(
+            packs, (break_offset, gains[0], cache_lengths), late_tokens, routes.T, experts + pad
+        )
+        factor = factor[:, :1]
         late_pieces, _ = gather(packed, masks[:-1])
         queries = (sum(part.astype(f32) for part in query_got) * factor).astype(bf16).astype(f32)
 
-        held = lax.optimization_barrier((queries, expert_gate, expert_up, expert_down))
-        queries, expert_gate, expert_up, expert_down = held
+        held = lax.optimization_barrier((query_part, expert_gate, expert_up, expert_down))
+        query_part, expert_gate, expert_up, expert_down = held
         gates, ups, downs = [[w, swap(w, 1)] for w in (expert_gate, expert_up, expert_down)]
         scaled = attend(
-            queries, past_keys, past_values, offsets, cache_lengths, gain_row, routed_mask
+            queries, past_keys, past_values, offsets, lengths, gain_row, routed_mask
         )
         held = lax.optimization_barrier((scaled, gates, ups, downs, late_pieces))
         scaled, gates, ups, downs, late_pieces = held
@@ -476,8 +514,8 @@
         residual_plane = jnp.concatenate([cut(residual_part, back_at[o], block) for o in range(inner)], axis=1)
         held = lax.optimization_barrier((residual_plane, gates, ups, downs, gained, shared))
         residual_plane, gates, ups, downs, gained, shared = held
-        held_weights = load_weights((*gates, *ups, *downs))
-        gates, ups, downs = held_weights[:2], held_weights[2:4], held_weights[4:]
+        loaded = load_weights((*gates, *ups, *downs))
+        gates, ups, downs = loaded[:2], loaded[2:4], loaded[4:]
         peers = outer_exchange([residual_plane] * outer)
         stacked = []
         for k in range(outer):
@@ -499,8 +537,6 @@
         router = router_weight.T
         results = []
         for i, piece in enumerate(row_pieces):
-            if i > 0:
-                piece, results = lax.optimization_barrier((piece, results))
             extra = shared if i == 0 else ()
             results.append(run_experts(piece, ffn_row, router, gates, ups, downs, place, cols, seqs, extra))
         sums = []

time: 89 us -> 89.3 us (level)
  waiting for transfers between devices: 22.4 us -> 29.1 us
  starting transfers between devices: 37.6 us -> 34.2 us
  other arithmetic: 3 us -> 1.27 us
  local copies, waits for them, and re-layouts: 4.18 us -> 2.95 us
    ppermute x3, waiting for transfers between devices: 1.15 us -> 5 us  [tp_swap(): return lax.ppermute(value, 'tp', [(i, (i + 1) % n_tp) for i in range(n_tp)])]
    ppermute x29, starting transfers between devices: 34 us -> 30.5 us  [swap(): return lax.ppermute(value, 'ep', [(i, i ^ mask) for i in range(n_ep)])]
    ppermute x29, waiting for transfers between devices: 21.2 us -> 24.1 us  [swap(): return lax.ppermute(value, 'ep', [(i, i ^ mask) for i in range(n_ep)])]
    reduce_sum x2 -> x0, other arithmetic: 1.73 us -> none  [the longest x1 0.97 us: body(): jnp.mean(wide_tokens * wide_tokens, axis=-1, keepdims=True) + epsilon]
  transfers between devices with their start and end apart: 32 -> 32, of which waited for: 12 -> 12; matrix products, arithmetic and copies ran while one was open for 6% -> 3% of each run, Pallas kernels for 20% -> 20%
where the time goes in v2:
time: 89.3 us; the launch traced here: 89 us
  starting transfers between devices  34.2 us (38%)
  waiting for transfers between devices  29.1 us (33%)
  Pallas kernels  20.4 us (23%)
  local copies, waits for them, and re-layouts  2.95 us (3%)
  other arithmetic  1.27 us (1%)
  between operations  1.08 us (1%)
    ppermute x29, starting transfers between devices, swap(): return lax.ppermute(value, 'ep', [(i, i ^ mask) for i in range(n_ep)])  30.5 us
    ppermute x29, waiting for transfers between devices, swap(): return lax.ppermute(value, 'ep', [(i, i ^ mask) for i in range(n_ep)])  24.1 us
    pallas_call x1, Pallas kernels, attend(): pl.pallas_call(kernel, out_shape=jax.ShapeDtypeStruct((seq_count, total),...  7.84 us
    pallas_call x3, Pallas kernels, load_weights(): pl.pallas_call(kernel, out_shape=tuple((pltpu.VMEM(w.shape, w.dtype) for...  5.66 us
    pallas_call x2, Pallas kernels, run_experts(): pl.pallas_call(kernel, out_shape=(jax.ShapeDtypeStruct((count, cols), f32...  5.01 us
    ppermute x3, waiting for transfers between devices, tp_swap(): return lax.ppermute(value, 'tp', [(i, (i + 1) % n_tp) for i in range(n_tp)])  5 us
    ppermute x3, starting transfers between devices, tp_swap(): return lax.ppermute(value, 'tp', [(i, (i + 1) % n_tp) for i in range(n_tp)])  3.74 us
  transfers between devices with their start and end apart: 32, of which 12 were waited for; matrix products, arithmetic and copies ran while one was open for 3% of the time, Pallas kernels for 20%

profile of v2, /device:TPU:0, one launch (start us, length us, event | category | flops | bytes accessed | tf_op | source)
XLA Modules:
  0.0 89.0 jit_solution(1906173186543873017)
XLA Ops:
  0.6 3.0 %collective-permute-start.3 = (bf16[128,512]{1,0:T(8,128)(2,1)}, bf16[128,512]{1,0:T(8,128)(2,1)S(1)}, u32[]{:S(2)}, u32[]{:S(2)}) collective-permute-start(bf16[128,512]{1,0:T(8,128)(2,1)} %refs_0_.2), channel_id=1, source_target_pairs={{0,4},{2,6},{4,0},{6,2},{8,12},{10,14},{12,8},{14,10},{16,20},{18,... | collective-permute-start | bytes 393224 | tf_op jit(solution)/shard_map/ppermute | solution.py:389
  4.6 1.6 %collective-permute-start = (bf16[16,512]{1,0:T(8,128)(2,1)S(1)}, bf16[16,512]{1,0:T(8,128)(2,1)S(1)}, u32[]{:S(2)}, u32[]{:S(2)}) collective-permute-start(bf16[16,512]{1,0:T(8,128)(2,1)S(1)} %get-tuple-element.185), channel_id=1, source_target_pairs={{0,8},{2,10},{4,12},{6,14},{8,0},{10,2},{12,4},{14,6},{16,24},{18,... | collective-permute-start | bytes 49160 | tf_op jit(solution)/shard_map/ppermute | solution.py:389
  6.3 2.6 %collective-permute-start.1 = (bf16[16,512]{1,0:T(8,128)(2,1)S(1)}, bf16[16,512]{1,0:T(8,128)(2,1)S(1)}, u32[]{:S(2)}, u32[]{:S(2)}) collective-permute-start(bf16[16,512]{1,0:T(8,128)(2,1)S(1)} %get-tuple-element.184), channel_id=1, source_target_pairs={{0,16},{2,18},{4,20},{6,22},{8,24},{10,26},{12,28},{14,30},{16,0},... | collective-permute-start | bytes 49160 | tf_op jit(solution)/shard_map/ppermute | solution.py:389
  11.0 3.4 %collective-permute-done.2 = bf16[16,512]{1,0:T(8,128)(2,1)S(1)} collective-permute-done((bf16[16,512]{1,0:T(8,128)(2,1)S(1)}, bf16[16,512]{1,0:T(8,128)(2,1)S(1)}, u32[]{:S(2)}, u32[]{:S(2)}) %collective-permute-start.2) | collective-permute-done | bytes 16416 | tf_op jit(solution)/shard_map/ppermute | solution.py:389
  18.9 1.8 %collective-permute-done.6 = bf16[16,512]{1,0:T(8,128)(2,1)S(1)} collective-permute-done((bf16[16,512]{1,0:T(8,128)(2,1)S(1)}, bf16[16,512]{1,0:T(8,128)(2,1)S(1)}, u32[]{:S(2)}, u32[]{:S(2)}) %collective-permute-start.6) | collective-permute-done | bytes 16416 | tf_op jit(solution)/shard_map/ppermute | solution.py:389
  20.6 1.9 %collective-permute-start.8 = (bf16[16,512]{1,0:T(8,128)(2,1)S(1)}, bf16[16,512]{1,0:T(8,128)(2,1)S(1)}, u32[]{:S(2)}, u32[]{:S(2)}) collective-permute-start(bf16[16,512]{1,0:T(8,128)(2,1)S(1)} %get-tuple-element.176), channel_id=1, source_target_pairs={{0,24},{2,26},{4,28},{6,30},{8,16},{10,18},{12,20},{14,22},{16,8},... | collective-permute-start | bytes 49160 | tf_op jit(solution)/shard_map/ppermute | solution.py:389
  23.3 2.9 %collective-permute-done.8 = bf16[16,512]{1,0:T(8,128)(2,1)S(1)} collective-permute-done((bf16[16,512]{1,0:T(8,128)(2,1)S(1)}, bf16[16,512]{1,0:T(8,128)(2,1)S(1)}, u32[]{:S(2)}, u32[]{:S(2)}) %collective-permute-start.8) | collective-permute-done | bytes 16416 | tf_op jit(solution)/shard_map/ppermute | solution.py:389
  26.3 7.8 %stick_attend.1.refs_0_ = bf16[16,768]{1,0:T(8,128)(2,1)S(1)} custom-call(s32[16]{0:T(128)S(1)} %get-tuple-element.98.refs_0_, f32[16,512]{1,0:T(8,128)S(1)} %fusion.4.refs_1_, bf16[16,2048,128]{2,1,0:T(8,128)(2,1)} %bitcast.10, bf16[16,2048,128]{2,1,0:T(8,128)(2,1)} %bitcast.11, f32[16,4,1024]{2,1,0:T(4,128)S(1)} %get-tuple-element.101.refs_4_, ...), custom_call_target="tpu_custom_call" | custom-call | flops 2000000000 | bytes 20000000 | tf_op jit(solution)/shard_map/stick_attend/pallas_call | solution.py:175
  34.8 2.4 %collective-permute-start.14 = (bf16[16,768]{1,0:T(8,128)(2,1)S(1)}, bf16[16,768]{1,0:T(8,128)(2,1)S(1)}, u32[]{:S(2)}, u32[]{:S(2)}) collective-permute-start(bf16[16,768]{1,0:T(8,128)(2,1)S(1)} %stick_attend.1.refs_0_), channel_id=1, source_target_pairs={{0,16},{2,18},{4,20},{6,22},{8,24},{10,26},{12,28},{14,30},{16,0},... | collective-permute-start | bytes 73736 | tf_op jit(solution)/shard_map/ppermute | solution.py:389
  37.1 2.0 %collective-permute-start.15 = (bf16[16,768]{1,0:T(8,128)(2,1)S(1)}, bf16[16,768]{1,0:T(8,128)(2,1)S(1)}, u32[]{:S(2)}, u32[]{:S(2)}) collective-permute-start(bf16[16,768]{1,0:T(8,128)(2,1)S(1)} %stick_attend.1.refs_0_), channel_id=1, source_target_pairs={{0,24},{2,26},{4,28},{6,30},{8,16},{10,18},{12,20},{14,22},{16,8},... | collective-permute-start | bytes 73736 | tf_op jit(solution)/shard_map/ppermute | solution.py:389
  39.5 3.3 %collective-permute-done.15.refs_3_ = bf16[16,768]{1,0:T(8,128)(2,1)S(1)} collective-permute-done((bf16[16,768]{1,0:T(8,128)(2,1)S(1)}, bf16[16,768]{1,0:T(8,128)(2,1)S(1)}, u32[]{:S(2)}, u32[]{:S(2)}) %collective-permute-start.15) | collective-permute-done | bytes 24608 | tf_op jit(solution)/shard_map/ppermute | solution.py:389
  44.7 1.9 %load_weights.4 = (bf16[2048,256]{1,0:T(8,128)(2,1)S(1)}, bf16[2048,256]{1,0:T(8,128)(2,1)S(1)}, bf16[256,2048]{1,0:T(8,128)(2,1)S(1)}) custom-call(bf16[2048,256]{1,0:T(8,128)(2,1)} %refs_0_.4, bf16[2048,256]{1,0:T(8,128)(2,1)} %refs_1_.1, bf16[256,2048]{1,0:T(8,128)(2,1)} %refs_2_.2), custom_call_target="tpu_custom_call" | custom-call | tf_op jit(solution)/shard_map/load_weights/pallas_call | solution.py:152
  48.0 2.6 %collective-permute-start.20 = (bf16[64,512]{1,0:T(8,128)(2,1)S(1)}, bf16[64,512]{1,0:T(8,128)(2,1)S(1)}, u32[]{:S(2)}, u32[]{:S(2)}) collective-permute-start(bf16[64,512]{1,0:T(8,128)(2,1)S(1)} %pad_maximum_fusion.2), channel_id=1, source_target_pairs={{0,16},{2,18},{4,20},{6,22},{8,24},{10,26},{12,28},{14,30},{16,0},... | collective-permute-start | bytes 196616 | tf_op jit(solution)/shard_map/ppermute | solution.py:389
  50.6 1.8 %collective-permute-start.21 = (bf16[64,512]{1,0:T(8,128)(2,1)S(1)}, bf16[64,512]{1,0:T(8,128)(2,1)S(1)}, u32[]{:S(2)}, u32[]{:S(2)}) collective-permute-start(bf16[64,512]{1,0:T(8,128)(2,1)S(1)} %pad_maximum_fusion.2), channel_id=1, source_target_pairs={{0,24},{2,26},{4,28},{6,30},{8,16},{10,18},{12,20},{14,22},{16,8},... | collective-permute-start | bytes 196616 | tf_op jit(solution)/shard_map/ppermute | solution.py:389
  52.4 2.9 %load_weights.5 = (bf16[1,2048,256]{2,1,0:T(8,128)(2,1)S(1)}, bf16[1,2048,256]{2,1,0:T(8,128)(2,1)S(1)}, bf16[1,2048,256]{2,1,0:T(8,128)(2,1)S(1)}, bf16[1,2048,...) custom-call(bf16[1,2048,256]{2,1,0:T(8,128)(2,1)} %refs_0_.5, ...), custom_call_target="tpu_custom_call" | custom-call | tf_op jit(solution)/shard_map/load_weights/pallas_call | solution.py:152
  57.4 6.0 %collective-permute-done.23.refs_1_ = bf16[64,2176]{1,0:T(8,128)(2,1)S(1)} collective-permute-done((bf16[64,2176]{1,0:T(8,128)(2,1)S(1)}, bf16[64,2176]{1,0:T(8,128)(2,1)S(1)}, u32[]{:S(2)}, u32[]{:S(2)}) %collective-permute-start.23) | collective-permute-done | bytes 278560 | tf_op jit(solution)/shard_map/ppermute | solution.py:389
  63.5 2.2 %routed_experts.3 = (f32[64,1024]{1,0:T(8,128)S(1)}, bf16[64,1024]{1,0:T(8,128)(2,1)S(1)}) custom-call(s32[4]{0:T(128)S(1)} %add_convert_fusion.1.refs_0_, bf16[64,2176]{1,0:T(8,128)(2,1)S(1)} %collective-permute-done.23.refs_1_, bf16[1,2048]{1,0:T(2,128)(2,1)S(1)} %reshape.73.refs_2_, bf16[16,2048]{1,0:T(8,128)(2,1)S(1)} %bitcast.8, ...), custom_call_target="tpu_custom_call" | custom-call | tf_op jit(solution)/shard_map/routed_experts/pallas_call | solution.py:361
  67.3 2.4 %collective-permute-start.30 = (bf16[16,512]{1,0:T(8,128)(2,1)S(1)}, bf16[16,512]{1,0:T(8,128)(2,1)S(1)}, u32[]{:S(2)}, u32[]{:S(2)}) collective-permute-start(bf16[16,512]{1,0:T(8,128)(2,1)S(1)} %get-tuple-element.170), channel_id=1, source_target_pairs={{0,16},{2,18},{4,20},{6,22},{8,24},{10,26},{12,28},{14,30},{16,0},... | collective-permute-start | bytes 49160 | tf_op jit(solution)/shard_map/ppermute | solution.py:389
  69.7 2.0 %collective-permute-start.31 = (bf16[16,512]{1,0:T(8,128)(2,1)S(1)}, bf16[16,512]{1,0:T(8,128)(2,1)S(1)}, u32[]{:S(2)}, u32[]{:S(2)}) collective-permute-start(bf16[16,512]{1,0:T(8,128)(2,1)S(1)} %get-tuple-element.169), channel_id=1, source_target_pairs={{0,24},{2,26},{4,28},{6,30},{8,16},{10,18},{12,20},{14,22},{16,8},... | collective-permute-start | bytes 49160 | tf_op jit(solution)/shard_map/ppermute | solution.py:389
  71.7 2.8 %routed_experts.2 = (f32[64,1024]{1,0:T(8,128)S(1)}, bf16[64,1024]{1,0:T(8,128)(2,1)S(1)}) custom-call(s32[4]{0:T(128)S(1)} %add_convert_fusion.1.refs_0_, bf16[64,2176]{1,0:T(8,128)(2,1)S(1)} %constant_dynamic-update-slice_fusion.11.refs_1_, bf16[1,2048]{1,0:T(2,128)(2,1)S(1)} %reshape.73.refs_2_, bf16[16,2048]{1,0:T(8,128)(2,1)S(1)} %bitcast.9, ...), custom_call_target="tpu_custom_call" | custom-call | tf_op jit(solution)/shard_map/routed_experts/pallas_call | solution.py:361
  75.5 4.0 %collective-permute-done.22 = bf16[64,1024]{1,0:T(8,128)(2,1)S(1)} collective-permute-done((bf16[64,1024]{1,0:T(8,128)(2,1)S(1)}, bf16[64,1024]{1,0:T(8,128)(2,1)S(1)}, u32[]{:S(2)}, u32[]{:S(2)}) %collective-permute-start.22) | collective-permute-done | bytes 131104 | tf_op jit(solution)/shard_map/ppermute | solution.py:401
  80.3 2.3 %collective-permute-start.27 = (bf16[16,1024]{1,0:T(8,128)(2,1)S(1)}, bf16[16,1024]{1,0:T(8,128)(2,1)S(1)}, u32[]{:S(2)}, u32[]{:S(2)}) collective-permute-start(bf16[16,1024]{1,0:T(8,128)(2,1)S(1)} %get-tuple-element.167), channel_id=1, source_target_pairs={{0,16},{2,18},{4,20},{6,22},{8,24},{10,26},{12,28},{14,30},{16,0},... | collective-permute-start | bytes 98312 | tf_op jit(solution)/shard_map/ppermute | solution.py:389
  82.6 2.0 %collective-permute-start.28 = (bf16[16,1024]{1,0:T(8,128)(2,1)S(1)}, bf16[16,1024]{1,0:T(8,128)(2,1)S(1)}, u32[]{:S(2)}, u32[]{:S(2)}) collective-permute-start(bf16[16,1024]{1,0:T(8,128)(2,1)S(1)} %get-tuple-element.166), channel_id=1, source_target_pairs={{0,24},{2,26},{4,28},{6,30},{8,16},{10,18},{12,20},{14,22},{16,8},... | collective-permute-start | bytes 98312 | tf_op jit(solution)/shard_map/ppermute | solution.py:389
  85.3 3.1 %collective-permute-done.28 = bf16[16,1024]{1,0:T(8,128)(2,1)S(1)} collective-permute-done((bf16[16,1024]{1,0:T(8,128)(2,1)S(1)}, bf16[16,1024]{1,0:T(8,128)(2,1)S(1)}, u32[]{:S(2)}, u32[]{:S(2)}) %collective-permute-start.28) | collective-permute-done | bytes 32800 | tf_op jit(solution)/shard_map/ppermute | solution.py:389
  (105 shorter events, 19.2 us)
Async XLA Ops:
  0.6 13.9 %collective-permute-start.3 = (bf16[128,512]{1,0:T(8,128)(2,1)}, bf16[128,512]{1,0:T(8,128)(2,1)S(1)}, u32[]{:S(2)}, u32[]{:S(2)}) collective-permute-start(bf16[128,512]{1,0:T(8,128)(2,1)} %refs_0_.2), channel_id=1, source_target_pairs={{0,4},{2,6},{4,0},{6,2},{8,12},{10,14},{12,8},{14,10},{16,20},{18,... | collective-permute-start | bytes 393224 | tf_op jit(solution)/shard_map/ppermute | solution.py:389
  3.7 11.0 %collective-permute-start.4 = (bf16[128,512]{1,0:T(8,128)(2,1)}, bf16[128,512]{1,0:T(8,128)(2,1)S(1)}, u32[]{:S(2)}, u32[]{:S(2)}) collective-permute-start(bf16[128,512]{1,0:T(8,128)(2,1)} %refs_0_.2), channel_id=1, source_target_pairs={{0,2},{2,0},{4,6},{6,4},{8,10},{10,8},{12,14},{14,12},{16,18},{18,... | collective-permute-start | bytes 393224 | tf_op jit(solution)/shard_map/ppermute | solution.py:389
  4.6 6.3 %collective-permute-start = (bf16[16,512]{1,0:T(8,128)(2,1)S(1)}, bf16[16,512]{1,0:T(8,128)(2,1)S(1)}, u32[]{:S(2)}, u32[]{:S(2)}) collective-permute-start(bf16[16,512]{1,0:T(8,128)(2,1)S(1)} %get-tuple-element.185), channel_id=1, source_target_pairs={{0,8},{2,10},{4,12},{6,14},{8,0},{10,2},{12,4},{14,6},{16,24},{18,... | collective-permute-start | bytes 49160 | tf_op jit(solution)/shard_map/ppermute | solution.py:389
  8.9 5.5 %collective-permute-start.2 = (bf16[16,512]{1,0:T(8,128)(2,1)S(1)}, bf16[16,512]{1,0:T(8,128)(2,1)S(1)}, u32[]{:S(2)}, u32[]{:S(2)}) collective-permute-start(bf16[16,512]{1,0:T(8,128)(2,1)S(1)} %get-tuple-element.183), channel_id=1, source_target_pairs={{0,24},{2,26},{4,28},{6,30},{8,16},{10,18},{12,20},{14,22},{16,8},... | collective-permute-start | bytes 49160 | tf_op jit(solution)/shard_map/ppermute | solution.py:389
  16.2 18.0 %collective-permute-start.10 = (bf16[1,2048,256]{2,1,0:T(8,128)(2,1)}, bf16[1,2048,256]{2,1,0:T(8,128)(2,1)S(1)}, u32[]{:S(2)}, u32[]{:S(2)}) collective-permute-start(bf16[1,2048,256]{2,1,0:T(8,128)(2,1)} %refs_2_.3), channel_id=1, source_target_pairs={{0,2},{2,0},{4,6},{6,4},{8,10},{10,8},{12,14},{14,12},{16,18},{18,... | collective-permute-start | bytes 3145736 | tf_op jit(solution)/shard_map/ppermute | solution.py:389
  16.4 17.8 %collective-permute-start.11 = (bf16[1,256,2048]{2,1,0:T(8,128)(2,1)}, bf16[1,256,2048]{2,1,0:T(8,128)(2,1)S(1)}, u32[]{:S(2)}, u32[]{:S(2)}) collective-permute-start(bf16[1,256,2048]{2,1,0:T(8,128)(2,1)} %refs_4_.1), channel_id=1, source_target_pairs={{0,2},{2,0},{4,6},{6,4},{8,10},{10,8},{12,14},{14,12},{16,18},{18,... | collective-permute-start | bytes 3145736 | tf_op jit(solution)/shard_map/ppermute | solution.py:389
  16.7 17.4 %collective-permute-start.9 = (bf16[1,2048,256]{2,1,0:T(8,128)(2,1)}, bf16[1,2048,256]{2,1,0:T(8,128)(2,1)S(1)}, u32[]{:S(2)}, u32[]{:S(2)}) collective-permute-start(bf16[1,2048,256]{2,1,0:T(8,128)(2,1)} %refs_0_.5), channel_id=1, source_target_pairs={{0,2},{2,0},{4,6},{6,4},{8,10},{10,8},{12,14},{14,12},{16,18},{18,... | collective-permute-start | bytes 3145736 | tf_op jit(solution)/shard_map/ppermute | solution.py:389
  16.9 5.7 %collective-permute-start.7 = (bf16[16,512]{1,0:T(8,128)(2,1)S(1)}, bf16[16,512]{1,0:T(8,128)(2,1)S(1)}, u32[]{:S(2)}, u32[]{:S(2)}) collective-permute-start(bf16[16,512]{1,0:T(8,128)(2,1)S(1)} %get-tuple-element.177), channel_id=1, source_target_pairs={{0,16},{2,18},{4,20},{6,22},{8,24},{10,26},{12,28},{14,30},{16,0},... | collective-permute-start | bytes 49160 | tf_op jit(solution)/shard_map/ppermute | solution.py:389
  20.6 5.5 %collective-permute-start.8 = (bf16[16,512]{1,0:T(8,128)(2,1)S(1)}, bf16[16,512]{1,0:T(8,128)(2,1)S(1)}, u32[]{:S(2)}, u32[]{:S(2)}) collective-permute-start(bf16[16,512]{1,0:T(8,128)(2,1)S(1)} %get-tuple-element.176), channel_id=1, source_target_pairs={{0,24},{2,26},{4,28},{6,30},{8,16},{10,18},{12,20},{14,22},{16,8},... | collective-permute-start | bytes 49160 | tf_op jit(solution)/shard_map/ppermute | solution.py:389
  22.7 11.5 %collective-permute-start.12 = (bf16[128,1024]{1,0:T(8,128)(2,1)S(1)}, bf16[128,1024]{1,0:T(8,128)(2,1)S(1)}, u32[]{:S(2)}, u32[]{:S(2)}) collective-permute-start(bf16[128,1024]{1,0:T(8,128)(2,1)S(1)} %get-tuple-element.109.refs_4_.refs_0_), channel_id=1, source_target_pairs={{0,4},{2,6},{4,0},{6,2},{8,12},{10,14},{12,8},{14,10},{16,20},{18,... | collective-permute-start | bytes 786440 | tf_op jit(solution)/shard_map/ppermute | solution.py:389
  34.2 8.6 %collective-permute-start.16 = (bf16[128,1024]{1,0:T(8,128)(2,1)S(1)}, bf16[128,1024]{1,0:T(8,128)(2,1)S(1)}, u32[]{:S(2)}, u32[]{:S(2)}) collective-permute-start(bf16[128,1024]{1,0:T(8,128)(2,1)S(1)} %get-tuple-element.109.refs_4_.refs_0_), channel_id=1, source_target_pairs={{0,2},{2,0},{4,6},{6,4},{8,10},{10,8},{12,14},{14,12},{16,18},{18,... | collective-permute-start | bytes 786440 | tf_op jit(solution)/shard_map/ppermute | solution.py:389
  34.3 8.5 %collective-permute-start.17 = (bf16[128,1024]{1,0:T(8,128)(2,1)S(1)}, bf16[128,1024]{1,0:T(8,128)(2,1)S(1)}, u32[]{:S(2)}, u32[]{:S(2)}) collective-permute-start(bf16[128,1024]{1,0:T(8,128)(2,1)S(1)} %collective-permute-done.12.refs_5_.refs_1_), channel_id=1, source_target_pairs={{0,2},{2,0},{4,6},{6,4},{8,10},{10,8},{12,14},{14,12},{16,18},{18,... | collective-permute-start | bytes 786440 | tf_op jit(solution)/shard_map/ppermute | solution.py:389
  37.1 5.6 %collective-permute-start.15 = (bf16[16,768]{1,0:T(8,128)(2,1)S(1)}, bf16[16,768]{1,0:T(8,128)(2,1)S(1)}, u32[]{:S(2)}, u32[]{:S(2)}) collective-permute-start(bf16[16,768]{1,0:T(8,128)(2,1)S(1)} %stick_attend.1.refs_0_), channel_id=1, source_target_pairs={{0,24},{2,26},{4,28},{6,30},{8,16},{10,18},{12,20},{14,22},{16,8},... | collective-permute-start | bytes 73736 | tf_op jit(solution)/shard_map/ppermute | solution.py:389
  48.0 7.3 %collective-permute-start.19 = (bf16[64,512]{1,0:T(8,128)(2,1)S(1)}, bf16[64,512]{1,0:T(8,128)(2,1)S(1)}, u32[]{:S(2)}, u32[]{:S(2)}) collective-permute-start(bf16[64,512]{1,0:T(8,128)(2,1)S(1)} %pad_maximum_fusion.2), channel_id=1, source_target_pairs={{0,8},{2,10},{4,12},{6,14},{8,0},{10,2},{12,4},{14,6},{16,24},{18,... | collective-permute-start | bytes 196616 | tf_op jit(solution)/shard_map/ppermute | solution.py:389
  48.0 7.3 %collective-permute-start.20 = (bf16[64,512]{1,0:T(8,128)(2,1)S(1)}, bf16[64,512]{1,0:T(8,128)(2,1)S(1)}, u32[]{:S(2)}, u32[]{:S(2)}) collective-permute-start(bf16[64,512]{1,0:T(8,128)(2,1)S(1)} %pad_maximum_fusion.2), channel_id=1, source_target_pairs={{0,16},{2,18},{4,20},{6,22},{8,24},{10,26},{12,28},{14,30},{16,0},... | collective-permute-start | bytes 196616 | tf_op jit(solution)/shard_map/ppermute | solution.py:389
  50.6 6.1 %collective-permute-start.21 = (bf16[64,512]{1,0:T(8,128)(2,1)S(1)}, bf16[64,512]{1,0:T(8,128)(2,1)S(1)}, u32[]{:S(2)}, u32[]{:S(2)}) collective-permute-start(bf16[64,512]{1,0:T(8,128)(2,1)S(1)} %pad_maximum_fusion.2), channel_id=1, source_target_pairs={{0,24},{2,26},{4,28},{6,30},{8,16},{10,18},{12,20},{14,22},{16,8},... | collective-permute-start | bytes 196616 | tf_op jit(solution)/shard_map/ppermute | solution.py:389
  56.9 6.6 %collective-permute-start.23 = (bf16[64,2176]{1,0:T(8,128)(2,1)S(1)}, bf16[64,2176]{1,0:T(8,128)(2,1)S(1)}, u32[]{:S(2)}, u32[]{:S(2)}) collective-permute-start(bf16[64,2176]{1,0:T(8,128)(2,1)S(1)} %constant_dynamic-update-slice_fusion.11.refs_1_), channel_id=1, source_target_pairs={{0,4},{2,6},{4,0},{6,2},{8,12},{10,14},{12,8},{14,10},{16,20},{18,... | collective-permute-start | bytes 835592 | tf_op jit(solution)/shard_map/ppermute | solution.py:389
  65.7 9.3 %collective-permute-start.24 = (bf16[64,1024]{1,0:T(8,128)(2,1)S(1)}, bf16[64,1024]{1,0:T(8,128)(2,1)S(1)}, u32[]{:S(2)}, u32[]{:S(2)}) collective-permute-start(bf16[64,1024]{1,0:T(8,128)(2,1)S(1)} %get-tuple-element.161), channel_id=1, source_target_pairs={{0,1},{1,0},{2,3},{3,2},{4,5},{5,4},{6,7},{7,6},{8,9},{9,8},{10,11... | collective-permute-start | bytes 393224 | tf_op jit(solution)/shard_map/ppermute | solution.py:401
  67.3 8.1 %collective-permute-start.29 = (bf16[16,512]{1,0:T(8,128)(2,1)S(1)}, bf16[16,512]{1,0:T(8,128)(2,1)S(1)}, u32[]{:S(2)}, u32[]{:S(2)}) collective-permute-start(bf16[16,512]{1,0:T(8,128)(2,1)S(1)} %get-tuple-element.168), channel_id=1, source_target_pairs={{0,8},{2,10},{4,12},{6,14},{8,0},{10,2},{12,4},{14,6},{16,24},{18,... | collective-permute-start | bytes 49160 | tf_op jit(solution)/shard_map/ppermute | solution.py:389
  67.3 8.1 %collective-permute-start.30 = (bf16[16,512]{1,0:T(8,128)(2,1)S(1)}, bf16[16,512]{1,0:T(8,128)(2,1)S(1)}, u32[]{:S(2)}, u32[]{:S(2)}) collective-permute-start(bf16[16,512]{1,0:T(8,128)(2,1)S(1)} %get-tuple-element.170), channel_id=1, source_target_pairs={{0,16},{2,18},{4,20},{6,22},{8,24},{10,26},{12,28},{14,30},{16,0},... | collective-permute-start | bytes 49160 | tf_op jit(solution)/shard_map/ppermute | solution.py:389
  69.7 5.8 %collective-permute-start.31 = (bf16[16,512]{1,0:T(8,128)(2,1)S(1)}, bf16[16,512]{1,0:T(8,128)(2,1)S(1)}, u32[]{:S(2)}, u32[]{:S(2)}) collective-permute-start(bf16[16,512]{1,0:T(8,128)(2,1)S(1)} %get-tuple-element.169), channel_id=1, source_target_pairs={{0,24},{2,26},{4,28},{6,30},{8,16},{10,18},{12,20},{14,22},{16,8},... | collective-permute-start | bytes 49160 | tf_op jit(solution)/shard_map/ppermute | solution.py:389
  74.5 5.0 %collective-permute-start.22 = (bf16[64,1024]{1,0:T(8,128)(2,1)S(1)}, bf16[64,1024]{1,0:T(8,128)(2,1)S(1)}, u32[]{:S(2)}, u32[]{:S(2)}) collective-permute-start(bf16[64,1024]{1,0:T(8,128)(2,1)S(1)} %get-tuple-element.159), channel_id=1, source_target_pairs={{0,1},{1,0},{2,3},{3,2},{4,5},{5,4},{6,7},{7,6},{8,9},{9,8},{10,11... | collective-permute-start | bytes 393224 | tf_op jit(solution)/shard_map/ppermute | solution.py:401
  80.2 5.1 %collective-permute-start.26 = (bf16[16,1024]{1,0:T(8,128)(2,1)S(1)}, bf16[16,1024]{1,0:T(8,128)(2,1)S(1)}, u32[]{:S(2)}, u32[]{:S(2)}) collective-permute-start(bf16[16,1024]{1,0:T(8,128)(2,1)S(1)} %get-tuple-element.165), channel_id=1, source_target_pairs={{0,8},{2,10},{4,12},{6,14},{8,0},{10,2},{12,4},{14,6},{16,24},{18,... | collective-permute-start | bytes 98312 | tf_op jit(solution)/shard_map/ppermute | solution.py:389
  82.6 5.7 %collective-permute-start.28 = (bf16[16,1024]{1,0:T(8,128)(2,1)S(1)}, bf16[16,1024]{1,0:T(8,128)(2,1)S(1)}, u32[]{:S(2)}, u32[]{:S(2)}) collective-permute-start(bf16[16,1024]{1,0:T(8,128)(2,1)S(1)} %get-tuple-element.166), channel_id=1, source_target_pairs={{0,24},{2,26},{4,28},{6,30},{8,16},{10,18},{12,20},{14,22},{16,8},... | collective-permute-start | bytes 98312 | tf_op jit(solution)/shard_map/ppermute | solution.py:389
  (13 other events, 140.7 us)
